TPU v7x, 128 devices: a whole 4x4x4 slice. The times are simulated.
128 devices in a mesh: ep: 32 (over z, y, core), tp: 4 (over x).
Axes of the slice: x: 4, y: 4, z: 4, core: 2. Of those that a mesh axis runs over, the one named last changes fastest.
Arguments:
- queries: bfloat16 [16384, 1024], P('ep', 'tp'), may hold values from -6 to 6
- key_rows: bfloat16 [16384, 512], P('ep', 'tp'), may hold values from -6 to 6
- value_rows: bfloat16 [16384, 512], P('ep', 'tp'), may hold values from -6 to 6
- forget_logit: float32 [8, 16384], P('tp', 'ep'), may hold values from -1 to 17
- out_weight: bfloat16 [1024, 2048], P('tp'), may hold values from -0.1875 to 0.1875
- out_gain: float32 [2048], replicated, may hold values from 0.1 to 1.9
- moe_input: bfloat16 [16384, 2048], P('ep'), may hold values from -6 to 6
- moe_gain: float32 [2048], replicated, may hold values from 0.1 to 1.9
- router_group: bfloat16 [2048, 4], replicated, may hold values from -2 to 2
- router_expert: bfloat16 [2048, 32], replicated, may hold values from -0.125 to 0.125
- route_group: int32 [16384], P('ep'), may hold values from 0 to 3
- route_pick: int32 [16384, 2], P('ep'), may hold values from 0 to 7, as said below
- expert_gate: bfloat16 [32, 2048, 1024], P('ep', None, 'tp'), may hold values from -0.125 to 0.125
- expert_up: bfloat16 [32, 2048, 1024], P('ep', None, 'tp'), may hold values from -0.125 to 0.125
- expert_down: bfloat16 [32, 1024, 2048], P('ep', 'tp'), may hold values from -42 to 42
Outputs:
- mixer_out: bfloat16 [16384, 2048], P(('ep', 'tp'))
- moe_out: bfloat16 [16384, 2048], P(('ep', 'tp'))
Inputs may be any that keep to these rules, and one draw needn't show every extreme that they name: `route_pick`: the two entries of a row differ.
All inputs are finite; a program needn't handle non-finite values.
Results may differ from a plain program's by a relative error of at most 0.013.
Values may be sent and summed in bfloat16 or wider, within the bound.
No kernel may reach another device: no remote copies, remote signals or barrier semaphores. Data moves between devices by JAX's collectives and lax.ppermute only.
A program may use at most 128 MiB of HBM per device.

v0:
```python
import functools
import math
import jax
import jax.numpy as jnp
from jax import lax
from jax.experimental import pallas as pl
from jax.experimental.pallas import tpu as pltpu
from jax.sharding import PartitionSpec as P

DH = 128
GROUPS = 4
BLOCK = 512
PLANE = 8
DEPTH = 4
ROOT = math.sqrt(DH)
LOG2E = 1.4426950408889634
SCALE = LOG2E / ROOT
QT = 256


def put_rows(stat, first, row, half):
    for h in range(2):
        rest = row[:, h * half : (h + 1) * half]
        for p in range(3):
            piece = rest.astype(jnp.bfloat16).astype(jnp.float32)
            stat[first + 3 * h + p : first + 3 * h + p + 1, :] = piece
            rest = rest - piece


def attend_kernel(
    pos_ref, q0, q1, q2, q3, kv_hbm, o0, o1, o2, o3,
    kv, raw, sems, wide, keys, values, even, odd, peak_even, peak_odd, top, gap, acc, stat,
):
    own, ahead = pos_ref[0], DEPTH - 1 - pos_ref[1]
    width = wide.shape[2]
    half = width // 2
    tiles = [slice(t * QT, (t + 1) * QT) for t in range(width // QT)]
    arriving = [pltpu.make_async_copy(q, raw.at[s], sems.at[s]) for s, q in enumerate((q0, q1, q2, q3))]
    arriving += [
        pltpu.make_async_copy(kv_hbm.at[b], kv.at[b], sems.at[DEPTH + b]) for b in range(PLANE)
    ]
    for c in arriving:
        c.start()
    top[...] = jnp.full_like(top, -1e30)
    acc[...] = jnp.zeros_like(acc)
    line = lax.broadcasted_iota(jnp.int32, (DH, width), 0)
    head = lax.broadcasted_iota(jnp.int32, (DH, width), 1) // half
    index = line % 8
    pick = (line < 16) & (index >= 3 * head) & (index < 3 * head + 3)
    picks = jnp.where(pick, -1.0, 0.0).astype(jnp.bfloat16)
    for s in range(DEPTH):
        arriving[s].wait()

    def turn(s, carry):
        turned = jnp.transpose(raw[s].astype(jnp.float32)).astype(jnp.bfloat16)
        for h in range(2):
            wide[s, :DH, h * half : (h + 1) * half] = turned[h * DH : (h + 1) * DH, :]
        wide[s, DH:, :] = picks
        return carry

    lax.fori_loop(0, ahead + 1, turn, 0)
    for b in range(PLANE):
        arriving[DEPTH + b].wait()
    sums = jnp.zeros((1, width), jnp.float32)
    first_total = None
    for b in reversed(range(PLANE)):
        gates = kv[b, BLOCK:, :]
        last = gates[:, DH:].astype(jnp.float32)
        total = jnp.concatenate(
            [
                jnp.broadcast_to(
                    last[8 + 3 * h : 9 + 3 * h, DH - 1 : DH]
                    + last[9 + 3 * h : 10 + 3 * h, DH - 1 : DH]
                    + last[10 + 3 * h : 11 + 3 * h, DH - 1 : DH],
                    (1, half),
                )
                for h in range(2)
            ],
            axis=1,
        )
        if b == PLANE - 1:
            first_total = total
        else:
            sums = sums + total
        gap[b] = sums

    def prepare(b, carry):
        gates = kv[b, BLOCK:, :]
        gates = jnp.concatenate([gates, jnp.zeros((DH - 16, 2 * DH), jnp.bfloat16)], axis=0)
        turned = jnp.transpose(gates.astype(jnp.float32)).astype(jnp.bfloat16)
        lane = lax.broadcasted_iota(jnp.int32, turned.shape, 1)
        zero = jnp.zeros_like(turned)
        keys[b, :, :DH] = kv[b, :BLOCK, :DH]
        keys[b, : 2 * DH, DH:] = jnp.where(lane < 8, turned, zero)
        keys[b, 2 * DH :, DH:] = jnp.where(lane < 8, zero, turned)
        for c in range(BLOCK // DH):
            values[b, :DH, c * DH : (c + 1) * DH] = kv[b, c * DH : (c + 1) * DH, DH:]
        values[b, DH:, :] = jnp.ones((16, BLOCK), jnp.bfloat16)
        return carry

    lax.fori_loop(0, PLANE, prepare, 0)
    steps = own + 1 + PLANE * ahead

    def place(n):
        m = jnp.maximum(n - (own + 1), 0)
        mine = n <= own
        s = jnp.where(mine, 0, jnp.minimum(1 + (m >> 3), DEPTH - 1))
        b = jnp.where(mine, own - n, PLANE - 1 - (m & 7))
        return s, b

    def score(s, b, t, into, peak, masked):
        scores = jnp.dot(keys[b], wide[s, :, tiles[t]], preferred_element_type=jnp.float32)
        if masked:
            key_at = lax.broadcasted_iota(jnp.int32, scores.shape, 0)
            query_at = lax.broadcasted_iota(jnp.int32, scores.shape, 1) + (t * QT) % half
            scores = jnp.where(key_at <= query_at, scores, -1e30)
        into[:, tiles[t]] = scores
        peak[:, tiles[t]] = jnp.max(scores, axis=0, keepdims=True)

    def absorb(s, b, dead, t, held, peak):
        cols = tiles[t]
        old = top[s, :, cols]
        shift = gap[b, :, cols] + dead
        new = jnp.maximum(old, peak[:, cols] + shift)
        top[s, :, cols] = new
        p = jnp.exp2(held[:, cols] * SCALE - (new - shift) * SCALE)
        part = jnp.dot(values[b], p.astype(jnp.bfloat16), preferred_element_type=jnp.float32)
        acc[s, :, cols] = acc[s, :, cols] * jnp.exp2((old - new) * SCALE) + part

    def phase(n, held, held_peak, into, into_peak):
        s, b = place(n)
        dead = jnp.where(n < steps, 0.0, -1e30)
        later_s, later_b = place(n + 1)
        for t in range(len(tiles)):
            score(later_s, later_b, t, into, into_peak, False)
            absorb(s, b, dead, t, held, held_peak)

    for t in range(len(tiles)):
        score(0, own, t, even, peak_even, True)

    def step(i, carry):
        phase(2 * i, even, peak_even, odd, peak_odd)
        phase(2 * i + 1, odd, peak_odd, even, peak_even)
        return carry

    lax.fori_loop(0, (steps + 1) >> 1, step, 0)
    for s, out in enumerate((o0, o1, o2, o3)):

        @pl.when(s <= ahead)
        def _():
            weight = acc[s, DH : DH + 1, :]
            mean = acc[s, :DH, :] / weight
            for h in range(2):
                out[h * DH : (h + 1) * DH, :] = mean[:, h * half : (h + 1) * half].astype(jnp.bfloat16)
            level = top[s] * SCALE + jnp.log(weight) * LOG2E
            if s == 0:
                level = level - gap[own] * SCALE
                passed = gap[0] - gap[own]
            else:
                level = level + first_total * SCALE
                passed = gap[0] + first_total
            stat[...] = jnp.zeros_like(stat)
            put_rows(stat, 0, level, half)
            put_rows(stat, 6, passed * SCALE, half)
            out[2 * DH :, :] = stat[...].astype(jnp.bfloat16)


def attend(pos, sets, kv):
    rows = sets[0].shape[0]
    width = 2 * rows
    return pl.pallas_call(
        attend_kernel,
        out_shape=[jax.ShapeDtypeStruct((2 * DH + 16, rows), jnp.bfloat16)] * DEPTH,
        in_specs=[pl.BlockSpec(memory_space=pltpu.SMEM)]
        + [pl.BlockSpec(memory_space=pltpu.HBM)] * (DEPTH + 1),
        out_specs=[pl.BlockSpec(memory_space=pltpu.VMEM)] * DEPTH,
        scratch_shapes=[
            pltpu.VMEM(kv.shape, jnp.bfloat16),
            pltpu.VMEM((DEPTH, rows, 2 * DH), jnp.bfloat16),
            pltpu.SemaphoreType.DMA((DEPTH + PLANE,)),
            pltpu.VMEM((DEPTH, 2 * DH, width), jnp.bfloat16),
            pltpu.VMEM((PLANE, BLOCK, 2 * DH), jnp.bfloat16),
            pltpu.VMEM((PLANE, DH + 16, BLOCK), jnp.bfloat16),
            pltpu.VMEM((BLOCK, width), jnp.float32),
            pltpu.VMEM((BLOCK, width), jnp.float32),
            pltpu.VMEM((1, width), jnp.float32),
            pltpu.VMEM((1, width), jnp.float32),
            pltpu.VMEM((DEPTH, 1, width), jnp.float32),
            pltpu.VMEM((PLANE, 1, width), jnp.float32),
            pltpu.VMEM((DEPTH, DH + 16, width), jnp.float32),
            pltpu.VMEM((16, rows), jnp.float32),
        ],
        cost_estimate=pl.CostEstimate(
            flops=9_000_000_000, bytes_accessed=4_000_000, transcendentals=16_000_000
        ),
    )(pos, *sets, kv)


def merge_kernel(pos_ref, p0, p1, p2, p3, w_ref, out_ref):
    depth = pos_ref[1]
    parts = (p0, p1, p2, p3)

    def read(ref, first):
        stat = ref[2 * DH :, :].astype(jnp.float32)
        return [
            sum(stat[first + 3 * h + p : first + 3 * h + p + 1, :] for p in range(3)) for h in range(2)
        ]

    merged = []
    passed = read(p0, 6)
    levels = [read(p0, 0)]
    for d in range(1, DEPTH):
        own = read(parts[d], 0)
        lost = jnp.where(d <= depth, 0.0, -1e30)
        levels.append([own[h] + passed[h] + lost for h in range(2)])
        more = read(parts[d], 6)
        passed = [passed[h] + more[h] for h in range(2)]
    for h in range(2):
        high = levels[0][h]
        for d in range(1, DEPTH):
            high = jnp.maximum(high, levels[d][h])
        weights = [jnp.exp2(levels[d][h] - high) for d in range(DEPTH)]
        total = weights[0] + weights[1] + weights[2] + weights[3]
        mixed = None
        for d in range(DEPTH):
            term = parts[d][h * DH : (h + 1) * DH, :].astype(jnp.float32) * (weights[d] / total)
            mixed = term if mixed is None else mixed + term
        merged.append(mixed)
    attended = jnp.transpose(jnp.concatenate(merged, axis=0)).astype(jnp.bfloat16)
    for n in range(0, out_ref.shape[1], 512):
        out_ref[:, n : n + 512] = jnp.dot(
            attended, w_ref[:, n : n + 512], preferred_element_type=jnp.float32
        ).astype(jnp.bfloat16)


def merge(pos, parts, w):
    rows = parts[0].shape[1]
    return pl.pallas_call(
        merge_kernel,
        out_shape=jax.ShapeDtypeStruct((rows, w.shape[1]), jnp.bfloat16),
        in_specs=[pl.BlockSpec(memory_space=pltpu.SMEM)]
        + [pl.BlockSpec(memory_space=pltpu.VMEM)] * (DEPTH + 1),
        out_specs=pl.BlockSpec(memory_space=pltpu.VMEM),
        cost_estimate=pl.CostEstimate(
            flops=2 * rows * w.shape[0] * w.shape[1], bytes_accessed=4_000_000, transcendentals=8 * rows
        ),
    )(pos, *parts, w)


def three(x):
    hi = lax.reduce_precision(x, 8, 7)
    mid = lax.reduce_precision(x - hi, 8, 7)
    return jnp.stack([hi, mid, x - hi - mid], axis=-2).astype(jnp.bfloat16)


def pack(keys, values, gates):
    turned = values.reshape(BLOCK // DH, DH, DH).transpose(0, 2, 1).reshape(BLOCK, DH)
    parts = three(gates * ROOT).reshape(6, 2, 2 * DH).transpose(1, 0, 2)
    parts = jnp.pad(parts, ((0, 0), (0, 2), (0, 0))).reshape(16, 2 * DH)
    return jnp.concatenate([jnp.concatenate([keys, turned], axis=1), parts], axis=0)


def hidden_kernel(count, x_hbm, *refs):
    weights, (out_ref, x_ref, both, sems) = refs[: 2 * count], refs[2 * count :]
    ff = both.shape[2] // 2
    copies = [pltpu.make_async_copy(x_hbm, x_ref, sems.at[2 * count])]
    for q in range(count):
        copies.append(pltpu.make_async_copy(weights[2 * q], both.at[q, :, :ff], sems.at[2 * q]))
        copies.append(pltpu.make_async_copy(weights[2 * q + 1], both.at[q, :, ff:], sems.at[2 * q + 1]))
    for c in copies:
        c.start()
    copies[0].wait()
    for q in range(count):
        copies[1 + 2 * q].wait()
        copies[2 + 2 * q].wait()
        for r in range(0, x_ref.shape[0], 256):
            lines = slice(r, r + 256)
            pre = jnp.dot(x_ref[lines, :], both[q], preferred_element_type=jnp.float32)
            gated, lifted = pre[:, :ff], pre[:, ff:]
            out_ref[lines, q * ff : (q + 1) * ff] = (gated * jax.nn.sigmoid(gated) * lifted).astype(
                jnp.bfloat16
            )


def hidden_units(x, weights):
    rows, width = x.shape
    count, ff = len(weights) // 2, weights[0].shape[1]
    return pl.pallas_call(
        functools.partial(hidden_kernel, count),
        out_shape=jax.ShapeDtypeStruct((rows, count * ff), jnp.bfloat16),
        in_specs=[pl.BlockSpec(memory_space=pltpu.HBM)] * (1 + len(weights)),
        out_specs=pl.BlockSpec(memory_space=pltpu.VMEM),
        scratch_shapes=[
            pltpu.VMEM((rows, width), jnp.bfloat16),
            pltpu.VMEM((count, width, 2 * ff), jnp.bfloat16),
            pltpu.SemaphoreType.DMA((1 + 2 * count,)),
        ],
        cost_estimate=pl.CostEstimate(
            flops=count * 4 * rows * width * ff,
            bytes_accessed=count * 4 * width * ff,
            transcendentals=rows * count * ff,
        ),
    )(x, *weights)


def down_kernel(count, hidden_hbm, *refs):
    weights, (out_hbm, hidden, down, out, sems) = refs[:count], refs[count:]
    ff = down.shape[0] // count
    pairs = [(hidden_hbm, hidden)]
    pairs += [(w, down.at[q * ff : (q + 1) * ff, :]) for q, w in enumerate(weights)]
    copies = [pltpu.make_async_copy(src, dst, sems.at[k]) for k, (src, dst) in enumerate(pairs)]
    for c in copies:
        c.start()
    for c in copies:
        c.wait()
    stores = []
    for n in range(0, out.shape[1], 256):
        cols = slice(n, n + 256)
        out[:, cols] = jnp.dot(hidden[...], down[:, cols], preferred_element_type=jnp.float32).astype(
            out.dtype
        )
        stores.append(
            pltpu.make_async_copy(
                out.at[:, cols], out_hbm.at[:, cols], sems.at[len(pairs) + len(stores)]
            )
        )
        stores[-1].start()
    for c in stores:
        c.wait()


def down_columns(hidden, weights):
    rows, count = hidden.shape[0], len(weights)
    ff, columns = weights[0].shape
    return pl.pallas_call(
        functools.partial(down_kernel, count),
        out_shape=jax.ShapeDtypeStruct((rows, columns), jnp.bfloat16),
        in_specs=[pl.BlockSpec(memory_space=pltpu.HBM)] * (1 + count),
        out_specs=pl.BlockSpec(memory_space=pltpu.HBM),
        scratch_shapes=[
            pltpu.VMEM((rows, count * ff), jnp.bfloat16),
            pltpu.VMEM((count * ff, columns), jnp.bfloat16),
            pltpu.VMEM((rows, columns), jnp.bfloat16),
            pltpu.SemaphoreType.DMA((1 + count + columns // 256,)),
        ],
        cost_estimate=pl.CostEstimate(
            flops=2 * rows * count * ff * columns,
            bytes_accessed=2 * count * ff * columns,
            transcendentals=0,
        ),
    )(hidden, *weights)


def shift(x, by):
    count = lax.axis_size("tp")
    return lax.ppermute(x, "tp", [(i, (i + by) % count) for i in range(count)])


def rms_scale(row_block, scale_gain):
    values = row_block.astype(jnp.float32)
    return (
        values * lax.rsqrt(jnp.mean(values * values, axis=-1, keepdims=True) + 1e-06) * scale_gain
    )


def inner(
    queries,
    key_rows,
    value_rows,
    forget_logit,
    out_weight,
    out_gain,
    moe_input,
    moe_gain,
    router_group,
    router_expert,
    route_group,
    route_pick,
    expert_gate,
    expert_up,
    expert_down,
):
    tp_count = lax.axis_size("tp")
    ep_count = lax.axis_size("ep")
    tp_index = lax.axis_index("tp")
    ep_index = lax.axis_index("ep")
    group_rows, width_model = moe_input.shape
    own_rows = group_rows // tp_count
    experts = ep_count
    per_group = experts // GROUPS
    capacity = tp_count * own_rows // experts
    slots = experts * capacity

    gate, up, down = expert_gate[0], expert_up[0], expert_down[0]
    cuts = (slice(0, SPLIT), slice(SPLIT, width_model))
    low = [down[:, c] for c in cuts]
    left_gate, right_up = shift(gate, 1), shift(up, -1)
    left_low = [shift(low[0], 1), shift(low[1], 1)]
    right_low = [shift(low[0], -1), shift(low[1], -1)]
    left_up, right_gate = shift(up, 1), shift(gate, -1)
    far_gate, far_up = shift(left_gate, 1), shift(right_up, -1)
    far_low = [shift(left_low[0], 1), shift(right_low[1], -1)]

    running = jnp.cumsum(jax.nn.log_sigmoid(forget_logit), axis=1)
    packed = pack(key_rows, value_rows, running)
    planes = [[z * PLANE + i for i in range(PLANE)] for z in range(ep_count // PLANE)]
    gathered = lax.all_gather(packed, "ep", axis=0, tiled=True, axis_index_groups=planes)
    gathered = gathered.reshape(PLANE, *packed.shape)
    place = jnp.stack([ep_index % PLANE, ep_index // PLANE])
    asked = [queries]
    for d in range(1, DEPTH):
        pairs = [(i, i - PLANE * d) for i in range(PLANE * d, ep_count)]
        asked.append(lax.ppermute(queries, "ep", pairs))
    answers = attend(place, asked, gathered)
    told = [answers[0]]
    for d in range(1, DEPTH):
        pairs = [(i, i + PLANE * d) for i in range(ep_count - PLANE * d)]
        told.append(lax.ppermute(answers[d], "ep", pairs))

    own_first = tp_index * own_rows
    own_group = lax.dynamic_slice_in_dim(route_group, own_first, own_rows, 0)
    own_pick = lax.dynamic_slice_in_dim(route_pick, own_first, own_rows, 0)
    chosen = own_group[:, None] * per_group + own_pick
    expert_hit = chosen[:, :, None] == jnp.arange(experts, dtype=jnp.int32)
    usage = jnp.any(expert_hit, axis=1).astype(jnp.bfloat16)
    line = jnp.arange(own_rows, dtype=jnp.int32)
    earlier = (line[None, :] < line[:, None]).astype(jnp.bfloat16)
    before = jnp.dot(earlier, usage, preferred_element_type=jnp.float32).astype(jnp.int32)
    ranks = jnp.sum(jnp.where(expert_hit, before[:, None, :], 0), axis=2)
    target = jnp.where(ranks < capacity, chosen * capacity + ranks, slots)
    normed = rms_scale(
        lax.dynamic_slice_in_dim(moe_input, own_first, own_rows, 0), moe_gain
    ).astype(jnp.bfloat16)
    slot_at = jnp.arange(slots, dtype=jnp.int32)[:, None]
    sent = ((slot_at == target[None, :, 0]) | (slot_at == target[None, :, 1])).astype(jnp.bfloat16)
    outgoing = jnp.dot(sent, normed, preferred_element_type=jnp.float32).astype(jnp.bfloat16)
    outgoing = outgoing.reshape(experts, capacity, width_model)
    arrived = lax.all_to_all(outgoing, "ep", split_axis=0, concat_axis=0, tiled=True)
    arrived = arrived.reshape(slots, width_model)

    hidden = hidden_units(
        arrived, (gate, up, left_gate, left_up, right_gate, right_up, far_gate, far_up)
    )
    mixer_term = merge(place, told, out_weight)
    mixer_term, far_low[1] = lax.optimization_barrier((mixer_term, far_low[1]))
    returned = []
    for k in range(2):
        results = down_columns(hidden, (low[k], left_low[k], right_low[k], far_low[k]))
        back = lax.all_to_all(
            results.reshape(experts, capacity, -1), "ep", split_axis=0, concat_axis=0, tiled=True
        )
        returned.append(back.reshape(slots, -1))
    mixer_summed = lax.psum_scatter(mixer_term, "tp", scatter_dimension=0, tiled=True)
    mixer_out = rms_scale(mixer_summed, out_gain).astype(jnp.bfloat16)

    mixer_out, returned[1] = lax.optimization_barrier((mixer_out, returned[1]))
    group_logits = jnp.dot(normed, router_group, preferred_element_type=jnp.float32)
    expert_logits = jnp.dot(normed, router_expert, preferred_element_type=jnp.float32)
    group_top = jnp.max(group_logits, axis=1, keepdims=True)
    group_exp = jnp.exp(group_logits - group_top)
    group_hit = jnp.arange(GROUPS, dtype=jnp.int32)[None, :] == own_group[:, None]
    group_share = jnp.sum(jnp.where(group_hit, group_exp, 0.0), axis=1) / jnp.sum(group_exp, axis=1)
    picked_logits = jnp.sum(jnp.where(expert_hit, expert_logits[:, None, :], 0.0), axis=2)
    shares = group_share[:, None] * jax.nn.sigmoid(picked_logits - picked_logits[:, ::-1])
    column = jnp.arange(slots, dtype=jnp.int32)[None, :]
    weight = jnp.where(column == target[:, :1], shares[:, :1], 0.0) + jnp.where(
        column == target[:, 1:], shares[:, 1:], 0.0
    )
    high = lax.reduce_precision(weight, 8, 7)
    both = jnp.concatenate([high, weight - high], axis=1).astype(jnp.bfloat16)
    moe_out = jnp.concatenate(
        [
            jnp.dot(both, jnp.concatenate([back, back], axis=0), preferred_element_type=jnp.float32)
            for back in returned
        ],
        axis=1,
    )
    return (mixer_out, moe_out.astype(jnp.bfloat16))


SPLIT = 768


def solution(mesh):
    in_specs = (
        P("ep", "tp"),
        P("ep", "tp"),
        P("ep", "tp"),
        P("tp", "ep"),
        P("tp", None),
        P(),
        P("ep", None),
        P(),
        P(),
        P(),
        P("ep"),
        P("ep", None),
        P("ep", None, "tp"),
        P("ep", None, "tp"),
        P("ep", "tp", None),
    )
    out_specs = (P(("ep", "tp"), None), P(("ep", "tp"), None))
    return jax.shard_map(inner, mesh=mesh, in_specs=in_specs, out_specs=out_specs, check_vma=False)
```

profile of v0, /device:TPU:0, one launch (start us, length us, event | category | flops | bytes accessed | tf_op | source)
XLA Modules:
  0.0 253.9 jit_solution(3199003324427823205)
XLA Ops:
  10.2 1.6 pad_maximum_fusion.1
  11.9 1.3 collective-permute-start
  15.8 1.7 collective-permute-start.8
  18.6 1.7 collective-permute-start.6
  24.4 10.5 %collective-permute-done.6.refs_2_ = bf16[256,1280]{1,0:T(8,128)(2,1)S(1)} collective-permute-done((bf16[256,1280]{1,0:T(8,128)(2,1)S(1)}, bf16[256,1280]{1,0:T(8,128)(2,1)S(1)}, u32[]{:S(2)}, u32[]{:S(2)}) %collective-permute-start.6) | collective-permute-done | bytes 655392 | tf_op jit(solution)/shard_map/ppermute | solution.py:356
  34.8 2.8 %collective-permute-start.7 = (bf16[256,1280]{1,0:T(8,128)(2,1)S(1)}, bf16[256,1280]{1,0:T(8,128)(2,1)S(1)}, u32[]{:S(2)}, u32[]{:S(2)}) collective-permute-start(bf16[256,1280]{1,0:T(8,128)(2,1)S(1)} %collective-permute-done.6.refs_2_), channel_id=1, source_target_pairs={{0,3},{1,0},{2,1},{3,2},{4,7},{5,4},{6,5},{7,6},{8,11},{9,8},{10,9... | collective-permute-start | bytes 1966088 | tf_op jit(solution)/shard_map/ppermute | solution.py:356
  37.7 2.2 all-gather.2.cloned.1.call-done
  39.9 23.7 %shard_map.158 = (bf16[272,512]{1,0:T(8,128)(2,1)}, bf16[272,512]{1,0:T(8,128)(2,1)}, bf16[272,512]{1,0:T(8,128)(2,1)}, bf16[272,512]{1,0:T(8,128)(2,1)}) custom-call(s32[2]{0:T(128)} %pad_add_fusion.pos_ref, bf16[512,256]{1,0:T(8,128)(2,1)} %q0.1, bf16[512,256]{1,0:T(8,128)(2,1)} %copy-done.14, bf16[512,256]{1,0:T(8,128)(2,1)} %copy-done.15, ...), custom_call_target="tpu_custom_call" | custom-call | flops 8999999488 | bytes 4000000 | tf_op jit(solution)/shard_map/pallas_call | solution.py:171
  63.6 1.3 collective-permute-start.3
  64.9 1.3 collective-permute-start.4
  66.2 1.3 collective-permute-start.5
  67.6 4.7 %collective-permute-done.3.p1 = bf16[272,512]{1,0:T(8,128)(2,1)S(1)} collective-permute-done((bf16[272,512]{1,0:T(8,128)(2,1)}, bf16[272,512]{1,0:T(8,128)(2,1)S(1)}, u32[]{:S(2)}, u32[]{:S(2)}) %collective-permute-start.3) | collective-permute-done | bytes 278560 | tf_op jit(solution)/shard_map/ppermute | solution.py:418
  72.3 2.7 %collective-permute-start.11 = (bf16[2048,256]{1,0:T(8,128)(2,1)}, bf16[2048,256]{1,0:T(8,128)(2,1)}, u32[]{:S(2)}, u32[]{:S(2)}) collective-permute-start(bf16[2048,256]{1,0:T(8,128)(2,1)} %bitcast.49), channel_id=1, source_target_pairs={{0,3},{1,0},{2,1},{3,2},{4,7},{5,4},{6,5},{7,6},{8,11},{9,8},{10,9... | collective-permute-start | bytes 3145736 | tf_op jit(solution)/shard_map/ppermute | solution.py:356
  75.0 2.8 %collective-permute-done.4.p2 = bf16[272,512]{1,0:T(8,128)(2,1)S(1)} collective-permute-done((bf16[272,512]{1,0:T(8,128)(2,1)}, bf16[272,512]{1,0:T(8,128)(2,1)S(1)}, u32[]{:S(2)}, u32[]{:S(2)}) %collective-permute-start.4) | collective-permute-done | bytes 278560 | tf_op jit(solution)/shard_map/ppermute | solution.py:418
  78.6 3.9 %shard_map.159 = bf16[512,2048]{1,0:T(8,128)(2,1)} custom-call(s32[2]{0:T(128)} %pad_add_fusion.pos_ref, bf16[272,512]{1,0:T(8,128)(2,1)} %get-tuple-element.10.p0, bf16[272,512]{1,0:T(8,128)(2,1)} %copy-done.5, bf16[272,512]{1,0:T(8,128)(2,1)} %copy-done.6, bf16[272,512]{1,0:T(8,128)(2,1)} %copy-done.7, bf16[256,2048]{1,0:T(8,128)(2,1)} %w_ref.1), custom_call_target="tpu_custom_call" | custom-call | flops 536870912 | bytes 4000000 | tf_op jit(solution)/shard_map/pallas_call | solution.py:238
  82.5 2.0 convolution_convert_fusion
  84.5 10.4 %all-to-all-start = ((bf16[32,16,2048]{2,1,0:T(8,128)(2,1)}), bf16[32,16,2048]{2,1,0:T(8,128)(2,1)S(1)}, u32[]{:S(2)}, u32[]{:S(2)}) async-start(bf16[32,16,2048]{2,1,0:T(8,128)(2,1)} %bitcast.11), calls=%async_computation.1 | async-start | bytes 4194304 | tf_op jit(solution)/shard_map/all_to_all | solution.py:438
  94.9 2.8 %collective-permute-start.10 = (bf16[2048,256]{1,0:T(8,128)(2,1)}, bf16[2048,256]{1,0:T(8,128)(2,1)S(1)}, u32[]{:S(2)}, u32[]{:S(2)}) collective-permute-start(bf16[2048,256]{1,0:T(8,128)(2,1)} %bitcast.47), channel_id=1, source_target_pairs={{0,3},{1,0},{2,1},{3,2},{4,7},{5,4},{6,5},{7,6},{8,11},{9,8},{10,9... | collective-permute-start | bytes 3145736 | tf_op jit(solution)/shard_map/ppermute | solution.py:356
  98.5 2.0 collective-permute-done.11.refs_5_
  100.5 3.7 %collective-permute-start.13 = (bf16[2048,256]{1,0:T(8,128)(2,1)}, bf16[2048,256]{1,0:T(8,128)(2,1)}, u32[]{:S(2)}, u32[]{:S(2)}) collective-permute-start(bf16[2048,256]{1,0:T(8,128)(2,1)} %collective-permute-done.11.refs_5_), channel_id=1, source_target_pairs={{0,3},{1,0},{2,1},{3,2},{4,7},{5,4},{6,5},{7,6},{8,11},{9,8},{10,9... | collective-permute-start | bytes 3145736 | tf_op jit(solution)/shard_map/ppermute | solution.py:356
  104.2 1.8 slice.36.refs_0_
  106.3 62.8 %collective-permute-done.15.refs_1_ = bf16[256,768]{1,0:T(8,128)(2,1)} collective-permute-done((bf16[256,768]{1,0:T(8,128)(2,1)}, bf16[256,768]{1,0:T(8,128)(2,1)}, u32[]{:S(2)}, u32[]{:S(2)}) %collective-permute-start.15) | collective-permute-done | bytes 393248 | tf_op jit(solution)/shard_map/ppermute | solution.py:356
  173.0 1.3 copy-done.2
  174.3 8.3 %shard_map.160.hidden_hbm = bf16[512,1024]{1,0:T(8,128)(2,1)} custom-call(bf16[512,2048]{1,0:T(8,128)(2,1)} %bitcast.36, bf16[2048,256]{1,0:T(8,128)(2,1)} %bitcast.48, bf16[2048,256]{1,0:T(8,128)(2,1)} %bitcast.51, bf16[2048,256]{1,0:T(8,128)(2,1)} %collective-permute-done.8.refs_2_, bf16[2048,256]{1,0:T(8,128)(2,1)} %copy-done.13, ...), custom_call_target="tpu_custom_call" | custom-call | flops 4294967296 | bytes 8388608 | tf_op jit(solution)/shard_map/pallas_call | solution.py:288
  182.6 13.2 %collective-permute-done.17.refs_3_ = bf16[256,768]{1,0:T(8,128)(2,1)} collective-permute-done((bf16[256,768]{1,0:T(8,128)(2,1)}, bf16[256,768]{1,0:T(8,128)(2,1)}, u32[]{:S(2)}, u32[]{:S(2)}) %collective-permute-start.17) | collective-permute-done | bytes 393248 | tf_op jit(solution)/shard_map/ppermute | solution.py:356
  195.9 3.5 %shard_map.162 = bf16[512,768]{1,0:T(8,128)(2,1)} custom-call(bf16[512,1024]{1,0:T(8,128)(2,1)} %shard_map.160.hidden_hbm, bf16[256,768]{1,0:T(8,128)(2,1)} %slice.36.refs_0_, bf16[256,768]{1,0:T(8,128)(2,1)} %collective-permute-done.15.refs_1_, bf16[256,768]{1,0:T(8,128)(2,1)} %collective-permute-done.16.refs_2_, ...), custom_call_target="tpu_custom_call" | custom-call | flops 805306368 | bytes 1572864 | tf_op jit(solution)/shard_map/pallas_call | solution.py:335
  199.4 7.2 %all-to-all-start.2 = ((bf16[32,16,768]{2,1,0:T(8,128)(2,1)}), bf16[32,16,768]{2,1,0:T(8,128)(2,1)S(1)}, u32[]{:S(2)}, u32[]{:S(2)}) async-start(bf16[32,16,768]{2,1,0:T(8,128)(2,1)} %bitcast.35), calls=%async_computation.3 | async-start | bytes 1572864 | tf_op jit(solution)/shard_map/all_to_all | solution.py:449
  207.1 4.5 %shard_map.161 = bf16[512,1280]{1,0:T(8,128)(2,1)} custom-call(bf16[512,1024]{1,0:T(8,128)(2,1)} %shard_map.160.hidden_hbm, bf16[256,1280]{1,0:T(8,128)(2,1)} %copy-done.1, bf16[256,1280]{1,0:T(8,128)(2,1)} %collective-permute-done.14.refs_1_, bf16[256,1280]{1,0:T(8,128)(2,1)} %copy-done.3, bf16[256,1280]{1,0:T(8,128)(2,1)} %copy-done.4), custom_call_target="tpu_custom_call" | custom-call | flops 1342177280 | bytes 2621440 | tf_op jit(solution)/shard_map/pallas_call | solution.py:335
  211.6 9.6 %all-to-all-done.2 = bf16[32,16,768]{2,1,0:T(8,128)(2,1)S(1)} async-done(((bf16[32,16,768]{2,1,0:T(8,128)(2,1)}), bf16[32,16,768]{2,1,0:T(8,128)(2,1)S(1)}, u32[]{:S(2)}, u32[]{:S(2)}) %all-to-all-start.2) | async-done | bytes 786464 | tf_op jit(solution)/shard_map/all_to_all | solution.py:449
  221.2 4.0 %all-to-all-start.1 = ((bf16[32,16,1280]{2,1,0:T(8,128)(2,1)}), bf16[32,16,1280]{2,1,0:T(8,128)(2,1)S(1)}, u32[]{:S(2)}, u32[]{:S(2)}) async-start(bf16[32,16,1280]{2,1,0:T(8,128)(2,1)} %bitcast.34), calls=%async_computation.2 | async-start | bytes 2621440 | tf_op jit(solution)/shard_map/all_to_all | solution.py:449
  227.0 2.0 fusion.16
  229.0 16.7 %all-to-all-done.1 = bf16[32,16,1280]{2,1,0:T(8,128)(2,1)S(1)} async-done(((bf16[32,16,1280]{2,1,0:T(8,128)(2,1)}), bf16[32,16,1280]{2,1,0:T(8,128)(2,1)S(1)}, u32[]{:S(2)}, u32[]{:S(2)}) %all-to-all-start.1) | async-done | bytes 1310752 | tf_op jit(solution)/shard_map/all_to_all | solution.py:449
  (99 shorter events, 20.2 us)
Async XLA Ops:
  7.2 98.8 %copy-start = (bf16[2048,32]{0,1:T(8,128)(2,1)S(1)}, bf16[2048,32]{0,1:T(8,128)(2,1)}, u32[]{:S(2)}) copy-start(bf16[2048,32]{0,1:T(8,128)(2,1)} %param.24) | copy-start | bytes 393220
  7.2 15.1 %copy-start.11 = (s32[512,2]{0,1:T(2,128)S(1)}, s32[512,2]{0,1:T(2,128)}, u32[]{:S(2)}) copy-start(s32[512,2]{0,1:T(2,128)} %param.26) | copy-start | bytes 12292
  7.2 15.1 %copy-start.9 = (f32[2048]{0:T(1024)S(1)}, f32[2048]{0:T(1024)}, u32[]{:S(2)}) copy-start(f32[2048]{0:T(1024)} %param.22) | copy-start | bytes 24580
  7.2 32.7 %all-gather.2.cloned.1.call-start = ((), (), s32[]{:S(2)}) async-start(), calls=%async_computation.4 | async-start | bytes 2433024 | tf_op jit(solution)/shard_map/all_gather | solution.py:407
  11.8 213.9 %reduce-scatter.2.cloned.1.call-start = ((), (), s32[]{:S(2)}) async-start(), calls=%async_computation.5 | async-start | bytes 2621440 | tf_op jit(solution)/shard_map/reduce_scatter | solution.py:453
  11.9 25.8 %collective-permute-start = (bf16[512,256]{1,0:T(8,128)(2,1)}, bf16[512,256]{1,0:T(8,128)(2,1)S(1)}, u32[]{:S(2)}, u32[]{:S(2)}) collective-permute-start(bf16[512,256]{1,0:T(8,128)(2,1)} %q0.1), channel_id=1, source_target_pairs={{32,0},{36,4},{40,8},{44,12},{48,16},{52,20},{56,24},{60,28},{64,3... | collective-permute-start | bytes 786440 | tf_op jit(solution)/shard_map/ppermute | solution.py:413
  13.2 24.5 %collective-permute-start.1 = (bf16[512,256]{1,0:T(8,128)(2,1)}, bf16[512,256]{1,0:T(8,128)(2,1)S(1)}, u32[]{:S(2)}, u32[]{:S(2)}) collective-permute-start(bf16[512,256]{1,0:T(8,128)(2,1)} %q0.1), channel_id=1, source_target_pairs={{64,0},{68,4},{72,8},{76,12},{80,16},{84,20},{88,24},{92,28},{96,3... | collective-permute-start | bytes 786440 | tf_op jit(solution)/shard_map/ppermute | solution.py:413
  14.5 23.2 %collective-permute-start.2 = (bf16[512,256]{1,0:T(8,128)(2,1)}, bf16[512,256]{1,0:T(8,128)(2,1)S(1)}, u32[]{:S(2)}, u32[]{:S(2)}) collective-permute-start(bf16[512,256]{1,0:T(8,128)(2,1)} %q0.1), channel_id=1, source_target_pairs={{96,0},{100,4},{104,8},{108,12},{112,16},{116,20},{120,24},{124,28... | collective-permute-start | bytes 786440 | tf_op jit(solution)/shard_map/ppermute | solution.py:413
  15.8 81.9 %collective-permute-start.8 = (bf16[2048,256]{1,0:T(8,128)(2,1)}, bf16[2048,256]{1,0:T(8,128)(2,1)}, u32[]{:S(2)}, u32[]{:S(2)}) collective-permute-start(bf16[2048,256]{1,0:T(8,128)(2,1)} %bitcast.46), channel_id=1, source_target_pairs={{0,1},{1,2},{2,3},{3,0},{4,5},{5,6},{6,7},{7,4},{8,9},{9,10},{10,1... | collective-permute-start | bytes 3145736 | tf_op jit(solution)/shard_map/ppermute | solution.py:356
  18.6 151.3 %copy-start.1 = (bf16[256,1280]{1,0:T(8,128)(2,1)}, bf16[256,1280]{1,0:T(8,128)(2,1)S(1)}, u32[]{:S(2)}) copy-start(bf16[256,1280]{1,0:T(8,128)(2,1)S(1)} %slice.35.refs_0_) | copy-start | bytes 1966084
  18.6 16.3 %collective-permute-start.6 = (bf16[256,1280]{1,0:T(8,128)(2,1)S(1)}, bf16[256,1280]{1,0:T(8,128)(2,1)S(1)}, u32[]{:S(2)}, u32[]{:S(2)}) collective-permute-start(bf16[256,1280]{1,0:T(8,128)(2,1)S(1)} %slice.35.refs_0_), channel_id=1, source_target_pairs={{0,3},{1,0},{2,1},{3,2},{4,7},{5,4},{6,5},{7,6},{8,11},{9,8},{10,9... | collective-permute-start | bytes 1966088 | tf_op jit(solution)/shard_map/ppermute | solution.py:356
  34.8 28.8 %copy-start.3 = (bf16[256,1280]{1,0:T(8,128)(2,1)}, bf16[256,1280]{1,0:T(8,128)(2,1)S(1)}, u32[]{:S(2)}) copy-start(bf16[256,1280]{1,0:T(8,128)(2,1)S(1)} %collective-permute-done.6.refs_2_) | copy-start | bytes 1966084
  34.8 47.6 %collective-permute-start.7 = (bf16[256,1280]{1,0:T(8,128)(2,1)S(1)}, bf16[256,1280]{1,0:T(8,128)(2,1)S(1)}, u32[]{:S(2)}, u32[]{:S(2)}) collective-permute-start(bf16[256,1280]{1,0:T(8,128)(2,1)S(1)} %collective-permute-done.6.refs_2_), channel_id=1, source_target_pairs={{0,3},{1,0},{2,1},{3,2},{4,7},{5,4},{6,5},{7,6},{8,11},{9,8},{10,9... | collective-permute-start | bytes 1966088 | tf_op jit(solution)/shard_map/ppermute | solution.py:356
  37.6 2.2 copy-start.14
  37.6 2.2 copy-start.15
  63.6 8.6 %collective-permute-start.3 = (bf16[272,512]{1,0:T(8,128)(2,1)}, bf16[272,512]{1,0:T(8,128)(2,1)S(1)}, u32[]{:S(2)}, u32[]{:S(2)}) collective-permute-start(bf16[272,512]{1,0:T(8,128)(2,1)} %get-tuple-element.11), channel_id=1, source_target_pairs={{0,32},{4,36},{8,40},{12,44},{16,48},{20,52},{24,56},{28,60},{32,6... | collective-permute-start | bytes 835592 | tf_op jit(solution)/shard_map/ppermute | solution.py:418
  64.9 12.8 %collective-permute-start.4 = (bf16[272,512]{1,0:T(8,128)(2,1)}, bf16[272,512]{1,0:T(8,128)(2,1)S(1)}, u32[]{:S(2)}, u32[]{:S(2)}) collective-permute-start(bf16[272,512]{1,0:T(8,128)(2,1)} %get-tuple-element.12), channel_id=1, source_target_pairs={{0,64},{4,68},{8,72},{12,76},{16,80},{20,84},{24,88},{28,92},{32,9... | collective-permute-start | bytes 835592 | tf_op jit(solution)/shard_map/ppermute | solution.py:418
  66.2 11.5 %collective-permute-start.5 = (bf16[272,512]{1,0:T(8,128)(2,1)}, bf16[272,512]{1,0:T(8,128)(2,1)S(1)}, u32[]{:S(2)}, u32[]{:S(2)}) collective-permute-start(bf16[272,512]{1,0:T(8,128)(2,1)} %get-tuple-element.13), channel_id=1, source_target_pairs={{0,96},{4,100},{8,104},{12,108},{16,112},{20,116},{24,120},{28,124... | collective-permute-start | bytes 835592 | tf_op jit(solution)/shard_map/ppermute | solution.py:418
  72.3 5.5 %copy-start.5 = (bf16[272,512]{1,0:T(8,128)(2,1)}, bf16[272,512]{1,0:T(8,128)(2,1)S(1)}, u32[]{:S(2)}) copy-start(bf16[272,512]{1,0:T(8,128)(2,1)S(1)} %collective-permute-done.3.p1) | copy-start | bytes 835588
  72.3 28.3 %collective-permute-start.11 = (bf16[2048,256]{1,0:T(8,128)(2,1)}, bf16[2048,256]{1,0:T(8,128)(2,1)}, u32[]{:S(2)}, u32[]{:S(2)}) collective-permute-start(bf16[2048,256]{1,0:T(8,128)(2,1)} %bitcast.49), channel_id=1, source_target_pairs={{0,3},{1,0},{2,1},{3,2},{4,7},{5,4},{6,5},{7,6},{8,11},{9,8},{10,9... | collective-permute-start | bytes 3145736 | tf_op jit(solution)/shard_map/ppermute | solution.py:356
  84.5 88.5 %all-to-all-start = ((bf16[32,16,2048]{2,1,0:T(8,128)(2,1)}), bf16[32,16,2048]{2,1,0:T(8,128)(2,1)S(1)}, u32[]{:S(2)}, u32[]{:S(2)}) async-start(bf16[32,16,2048]{2,1,0:T(8,128)(2,1)} %bitcast.11), calls=%async_computation.1 | async-start | bytes 4194304 | tf_op jit(solution)/shard_map/all_to_all | solution.py:438
  94.9 75.0 %collective-permute-start.10 = (bf16[2048,256]{1,0:T(8,128)(2,1)}, bf16[2048,256]{1,0:T(8,128)(2,1)S(1)}, u32[]{:S(2)}, u32[]{:S(2)}) collective-permute-start(bf16[2048,256]{1,0:T(8,128)(2,1)} %bitcast.47), channel_id=1, source_target_pairs={{0,3},{1,0},{2,1},{3,2},{4,7},{5,4},{6,5},{7,6},{8,11},{9,8},{10,9... | collective-permute-start | bytes 3145736 | tf_op jit(solution)/shard_map/ppermute | solution.py:356
  97.7 73.4 %collective-permute-start.9 = (bf16[2048,256]{1,0:T(8,128)(2,1)}, bf16[2048,256]{1,0:T(8,128)(2,1)S(1)}, u32[]{:S(2)}, u32[]{:S(2)}) collective-permute-start(bf16[2048,256]{1,0:T(8,128)(2,1)} %bitcast.50), channel_id=1, source_target_pairs={{0,1},{1,2},{2,3},{3,0},{4,5},{5,6},{6,7},{7,4},{8,9},{9,10},{10,1... | collective-permute-start | bytes 3145736 | tf_op jit(solution)/shard_map/ppermute | solution.py:356
  97.7 75.3 %collective-permute-start.12 = (bf16[2048,256]{1,0:T(8,128)(2,1)}, bf16[2048,256]{1,0:T(8,128)(2,1)}, u32[]{:S(2)}, u32[]{:S(2)}) collective-permute-start(bf16[2048,256]{1,0:T(8,128)(2,1)} %collective-permute-done.8.refs_2_), channel_id=1, source_target_pairs={{0,1},{1,2},{2,3},{3,0},{4,5},{5,6},{6,7},{7,4},{8,9},{9,10},{10,1... | collective-permute-start | bytes 3145736 | tf_op jit(solution)/shard_map/ppermute | solution.py:356
  100.5 72.5 %collective-permute-start.13 = (bf16[2048,256]{1,0:T(8,128)(2,1)}, bf16[2048,256]{1,0:T(8,128)(2,1)}, u32[]{:S(2)}, u32[]{:S(2)}) collective-permute-start(bf16[2048,256]{1,0:T(8,128)(2,1)} %collective-permute-done.11.refs_5_), channel_id=1, source_target_pairs={{0,3},{1,0},{2,1},{3,2},{4,7},{5,4},{6,5},{7,6},{8,11},{9,8},{10,9... | collective-permute-start | bytes 3145736 | tf_op jit(solution)/shard_map/ppermute | solution.py:356
  106.0 63.0 %collective-permute-start.15 = (bf16[256,768]{1,0:T(8,128)(2,1)}, bf16[256,768]{1,0:T(8,128)(2,1)}, u32[]{:S(2)}, u32[]{:S(2)}) collective-permute-start(bf16[256,768]{1,0:T(8,128)(2,1)} %slice.36.refs_0_), channel_id=1, source_target_pairs={{0,1},{1,2},{2,3},{3,0},{4,5},{5,6},{6,7},{7,4},{8,9},{9,10},{10,1... | collective-permute-start | bytes 1179656 | tf_op jit(solution)/shard_map/ppermute | solution.py:356
  169.0 13.6 %collective-permute-start.16 = (bf16[256,768]{1,0:T(8,128)(2,1)}, bf16[256,768]{1,0:T(8,128)(2,1)}, u32[]{:S(2)}, u32[]{:S(2)}) collective-permute-start(bf16[256,768]{1,0:T(8,128)(2,1)} %slice.36.refs_0_), channel_id=1, source_target_pairs={{0,3},{1,0},{2,1},{3,2},{4,7},{5,4},{6,5},{7,6},{8,11},{9,8},{10,9... | collective-permute-start | bytes 1179656 | tf_op jit(solution)/shard_map/ppermute | solution.py:356
  169.9 37.2 %collective-permute-start.14 = (bf16[256,1280]{1,0:T(8,128)(2,1)S(1)}, bf16[256,1280]{1,0:T(8,128)(2,1)}, u32[]{:S(2)}, u32[]{:S(2)}) collective-permute-start(bf16[256,1280]{1,0:T(8,128)(2,1)S(1)} %slice.35.refs_0_), channel_id=1, source_target_pairs={{0,1},{1,2},{2,3},{3,0},{4,5},{5,6},{6,7},{7,4},{8,9},{9,10},{10,1... | collective-permute-start | bytes 1966088 | tf_op jit(solution)/shard_map/ppermute | solution.py:356
  172.1 23.8 %collective-permute-start.17 = (bf16[256,768]{1,0:T(8,128)(2,1)}, bf16[256,768]{1,0:T(8,128)(2,1)}, u32[]{:S(2)}, u32[]{:S(2)}) collective-permute-start(bf16[256,768]{1,0:T(8,128)(2,1)} %collective-permute-done.15.refs_1_), channel_id=1, source_target_pairs={{0,1},{1,2},{2,3},{3,0},{4,5},{5,6},{6,7},{7,4},{8,9},{9,10},{10,1... | collective-permute-start | bytes 1179656 | tf_op jit(solution)/shard_map/ppermute | solution.py:356
  182.6 24.1 %copy-start.8 = (bf16[2048,4]{0,1:T(4,128)(2,1)S(1)}, bf16[2048,4]{0,1:T(4,128)(2,1)}, u32[]{:S(2)}) copy-start(bf16[2048,4]{0,1:T(4,128)(2,1)} %param.23) | copy-start | bytes 49156
  199.4 21.8 %all-to-all-start.2 = ((bf16[32,16,768]{2,1,0:T(8,128)(2,1)}), bf16[32,16,768]{2,1,0:T(8,128)(2,1)S(1)}, u32[]{:S(2)}, u32[]{:S(2)}) async-start(bf16[32,16,768]{2,1,0:T(8,128)(2,1)} %bitcast.35), calls=%async_computation.3 | async-start | bytes 1572864 | tf_op jit(solution)/shard_map/all_to_all | solution.py:449
  221.2 24.5 %all-to-all-start.1 = ((bf16[32,16,1280]{2,1,0:T(8,128)(2,1)}), bf16[32,16,1280]{2,1,0:T(8,128)(2,1)S(1)}, u32[]{:S(2)}, u32[]{:S(2)}) async-start(bf16[32,16,1280]{2,1,0:T(8,128)(2,1)} %bitcast.34), calls=%async_computation.2 | async-start | bytes 2621440 | tf_op jit(solution)/shard_map/all_to_all | solution.py:449
  (8 other events, 11.1 us)
Sparse Core Ops, SparseCore 0:
  11.9 27.8 all-gather.1
  82.6 49.3 reduce-scatter.1
where the time goes:
time: 255 us; the launch traced here: 254 us
  waiting for transfers between devices  125 us (49%)
  starting transfers between devices  48.5 us (19%)
  Pallas kernels  44 us (17%)
  between operations  14.4 us (6%)
  other arithmetic  11.6 us (5%)
  local copies, waits for them, and re-layouts  7.31 us (3%)
  matrix products  3.57 us (1%)
    ppermute x12, waiting for transfers between devices, shift(): return lax.ppermute(x, 'tp', [(i, (i + by) % count) for i in range(count)])  88.5 us
    all_to_all x2, waiting for transfers between devices, inner(): lax.all_to_all(results.reshape(experts, capacity, -1), 'ep', split_axis=0...  26.3 us
    pallas_call x1, Pallas kernels, attend(): pl.pallas_call(attend_kernel, out_shape=[jax.ShapeDtypeStruct((2 * DH + 1...  23.7 us
    ppermute x12, starting transfers between devices, shift(): return lax.ppermute(x, 'tp', [(i, (i + by) % count) for i in range(count)])  19.1 us
    all_to_all x2, starting transfers between devices, inner(): lax.all_to_all(results.reshape(experts, capacity, -1), 'ep', split_axis=0...  11.2 us
    all_to_all x1, starting transfers between devices, inner(): lax.all_to_all(outgoing, 'ep', split_axis=0, concat_axis=0, tiled=True)  10.4 us
    pallas_call x1, Pallas kernels, hidden_units(): pl.pallas_call(functools.partial(hidden_kernel, count), out_shape=jax.Sha...  8.26 us
    pallas_call x2, Pallas kernels, down_columns(): pl.pallas_call(functools.partial(down_kernel, count), out_shape=jax.Shape...  8.05 us
  transfers between devices with their start and end apart: 23, of which 9 were waited for; matrix products, arithmetic and copies ran while one was open for 5% of the time, Pallas kernels for 17%

commit v1 on v0

--- a/solution.py
+++ b/solution.py
@@ -392,14 +392,20 @@
     slots = experts * capacity
 
     gate, up, down = expert_gate[0], expert_up[0], expert_down[0]
-    cuts = (slice(0, SPLIT), slice(SPLIT, width_model))
-    low = [down[:, c] for c in cuts]
+    half = gate.shape[1] // 2
+    low, low_a, low_b = down[:, :SPLIT], down[:half, SPLIT:], down[half:, SPLIT:]
     left_gate, right_up = shift(gate, 1), shift(up, -1)
-    left_low = [shift(low[0], 1), shift(low[1], 1)]
-    right_low = [shift(low[0], -1), shift(low[1], -1)]
+    left_low, right_low = shift(low, 1), shift(low, -1)
+    left_a, right_a = shift(low_a, 1), shift(low_a, -1)
+    left_b, right_b = shift(low_b, 1), shift(low_b, -1)
     left_up, right_gate = shift(up, 1), shift(gate, -1)
     far_gate, far_up = shift(left_gate, 1), shift(right_up, -1)
-    far_low = [shift(left_low[0], 1), shift(right_low[1], -1)]
+    far_low = shift(left_low, 1)
+    far_a, far_b = shift(right_a, -1), shift(left_b, 1)
+    lows = (
+        (low, left_low, right_low, far_low),
+        (low_a, low_b, left_a, left_b, right_a, right_b, far_a, far_b),
+    )
 
     running = jnp.cumsum(jax.nn.log_sigmoid(forget_logit), axis=1)
     packed = pack(key_rows, value_rows, running)
@@ -442,10 +448,9 @@
         arrived, (gate, up, left_gate, left_up, right_gate, right_up, far_gate, far_up)
     )
     mixer_term = merge(place, told, out_weight)
-    mixer_term, far_low[1] = lax.optimization_barrier((mixer_term, far_low[1]))
     returned = []
     for k in range(2):
-        results = down_columns(hidden, (low[k], left_low[k], right_low[k], far_low[k]))
+        results = down_columns(hidden, lows[k])
         back = lax.all_to_all(
             results.reshape(experts, capacity, -1), "ep", split_axis=0, concat_axis=0, tiled=True
         )

time: 255 us -> 261 us (1.024)
  starting transfers between devices: 48.5 us -> 52 us
    all_to_all x2, waiting for transfers between devices: 26.3 us -> 16.7 us  [inner(): lax.all_to_all(results.reshape(experts, capacity, -1), 'ep', split_axis=0...]
    ppermute x3, waiting for transfers between devices: 0.01 us -> 7.42 us  [inner(): asked.append(lax.ppermute(queries, 'ep', pairs))]
    all_gather x1, waiting for transfers between devices: 2.18 us -> 8.79 us  [inner(): lax.all_gather(packed, 'ep', axis=0, tiled=True, axis_index_groups=planes)]
    ppermute x12 -> x15, waiting for transfers between devices: 88.5 us -> 83 us  [shift(): return lax.ppermute(x, 'tp', [(i, (i + by) % count) for i in range(count)])]
    all_to_all x2, starting transfers between devices: 11.2 us -> 14.5 us  [inner(): lax.all_to_all(results.reshape(experts, capacity, -1), 'ep', split_axis=0...]
    ppermute x12 -> x15, starting transfers between devices: 19.1 us -> 19.4 us  [shift(): return lax.ppermute(x, 'tp', [(i, (i + by) % count) for i in range(count)])]
  transfers between devices with their start and end apart: 23 -> 26, of which waited for: 9 -> 10; matrix products, arithmetic and copies ran while one was open for 5% -> 6% of each run, Pallas kernels for 17% -> 17%
where the time goes in v1:
time: 261 us; the launch traced here: 260 us
  waiting for transfers between devices  125 us (48%)
  starting transfers between devices  52 us (20%)
  Pallas kernels  44 us (17%)
  between operations  14.4 us (6%)
  other arithmetic  12.9 us (5%)
  local copies, waits for them, and re-layouts  8.07 us (3%)
  matrix products  3.56 us (1%)
    ppermute x15, waiting for transfers between devices, shift(): return lax.ppermute(x, 'tp', [(i, (i + by) % count) for i in range(count)])  83 us
    pallas_call x1, Pallas kernels, attend(): pl.pallas_call(attend_kernel, out_shape=[jax.ShapeDtypeStruct((2 * DH + 1...  23.8 us
    ppermute x15, starting transfers between devices, shift(): return lax.ppermute(x, 'tp', [(i, (i + by) % count) for i in range(count)])  19.4 us
    all_to_all x2, waiting for transfers between devices, inner(): lax.all_to_all(results.reshape(experts, capacity, -1), 'ep', split_axis=0...  16.7 us
    all_to_all x2, starting transfers between devices, inner(): lax.all_to_all(results.reshape(experts, capacity, -1), 'ep', split_axis=0...  14.5 us
    all_to_all x1, starting transfers between devices, inner(): lax.all_to_all(outgoing, 'ep', split_axis=0, concat_axis=0, tiled=True)  10.2 us
    ppermute x3, waiting for transfers between devices, inner(): told.append(lax.ppermute(answers[d], 'ep', pairs))  9.49 us
    all_gather x1, waiting for transfers between devices, inner(): lax.all_gather(packed, 'ep', axis=0, tiled=True, axis_index_groups=planes)  8.79 us
  transfers between devices with their start and end apart: 26, of which 10 were waited for; matrix products, arithmetic and copies ran while one was open for 6% of the time, Pallas kernels for 17%

profile of v1, /device:TPU:0, one launch (start us, length us, event | category | flops | bytes accessed | tf_op | source)
XLA Modules:
  0.0 260.2 jit_solution(18256892893074717921)
XLA Ops:
  10.2 1.6 pad_maximum_fusion.1
  15.8 1.7 collective-permute-start.6
  17.4 1.6 collective-permute-start.9
  23.8 1.9 collective-permute-done.1.q2
  25.7 5.5 %collective-permute-done.2.q3 = bf16[512,256]{1,0:T(8,128)(2,1)S(1)} collective-permute-done((bf16[512,256]{1,0:T(8,128)(2,1)}, bf16[512,256]{1,0:T(8,128)(2,1)S(1)}, u32[]{:S(2)}, u32[]{:S(2)}) %collective-permute-start.2) | collective-permute-done | bytes 262176 | tf_op jit(solution)/shard_map/ppermute | solution.py:419
  31.2 8.8 %all-gather.2.cloned.1.call-done = bf16[4224,256]{1,0:T(8,128)(2,1)} async-done(((bf16[528,256]{1,0:T(8,128)(2,1)}), bf16[4224,256]{1,0:T(8,128)(2,1)}) %all-gather.2.cloned.1.call-update) | async-done | bytes 2162704 | tf_op jit(solution)/shard_map/all_gather | solution.py:413
  40.0 23.8 %shard_map.158 = (bf16[272,512]{1,0:T(8,128)(2,1)}, bf16[272,512]{1,0:T(8,128)(2,1)}, bf16[272,512]{1,0:T(8,128)(2,1)}, bf16[272,512]{1,0:T(8,128)(2,1)}) custom-call(s32[2]{0:T(128)} %pad_add_fusion.pos_ref, bf16[512,256]{1,0:T(8,128)(2,1)} %q0.1, bf16[512,256]{1,0:T(8,128)(2,1)} %copy-done.16, bf16[512,256]{1,0:T(8,128)(2,1)} %copy-done.17, ...), custom_call_target="tpu_custom_call" | custom-call | flops 8999999488 | bytes 4000000 | tf_op jit(solution)/shard_map/pallas_call | solution.py:171
  63.8 1.3 collective-permute-start.3
  65.1 1.3 collective-permute-start.4
  66.4 1.3 collective-permute-start.5
  68.4 4.0 %collective-permute-done.3.p1 = bf16[272,512]{1,0:T(8,128)(2,1)S(1)} collective-permute-done((bf16[272,512]{1,0:T(8,128)(2,1)}, bf16[272,512]{1,0:T(8,128)(2,1)S(1)}, u32[]{:S(2)}, u32[]{:S(2)}) %collective-permute-start.3) | collective-permute-done | bytes 278560 | tf_op jit(solution)/shard_map/ppermute | solution.py:424
  72.4 5.5 %collective-permute-done.4.p2 = bf16[272,512]{1,0:T(8,128)(2,1)S(1)} collective-permute-done((bf16[272,512]{1,0:T(8,128)(2,1)}, bf16[272,512]{1,0:T(8,128)(2,1)S(1)}, u32[]{:S(2)}, u32[]{:S(2)}) %collective-permute-start.4) | collective-permute-done | bytes 278560 | tf_op jit(solution)/shard_map/ppermute | solution.py:424
  78.7 3.9 %shard_map.159 = bf16[512,2048]{1,0:T(8,128)(2,1)} custom-call(s32[2]{0:T(128)} %pad_add_fusion.pos_ref, bf16[272,512]{1,0:T(8,128)(2,1)} %get-tuple-element.8.p0, bf16[272,512]{1,0:T(8,128)(2,1)} %copy-done.7, bf16[272,512]{1,0:T(8,128)(2,1)} %copy-done.8, bf16[272,512]{1,0:T(8,128)(2,1)} %copy-done.9, bf16[256,2048]{1,0:T(8,128)(2,1)} %w_ref.1), custom_call_target="tpu_custom_call" | custom-call | flops 536870912 | bytes 4000000 | tf_op jit(solution)/shard_map/pallas_call | solution.py:238
  82.7 2.0 convolution_convert_fusion
  84.7 10.2 %all-to-all-start = ((bf16[32,16,2048]{2,1,0:T(8,128)(2,1)}), bf16[32,16,2048]{2,1,0:T(8,128)(2,1)S(1)}, u32[]{:S(2)}, u32[]{:S(2)}) async-start(bf16[32,16,2048]{2,1,0:T(8,128)(2,1)} %bitcast.10), calls=%async_computation.1 | async-start | bytes 4194304 | tf_op jit(solution)/shard_map/all_to_all | solution.py:444
  94.9 1.5 collective-permute-start.7
  96.5 1.8 collective-permute-start.8
  98.5 3.0 %collective-permute-start.11 = (bf16[2048,256]{1,0:T(8,128)(2,1)}, bf16[2048,256]{1,0:T(8,128)(2,1)S(1)}, u32[]{:S(2)}, u32[]{:S(2)}) collective-permute-start(bf16[2048,256]{1,0:T(8,128)(2,1)} %collective-permute-done.9.refs_5_), channel_id=1, source_target_pairs={{0,3},{1,0},{2,1},{3,2},{4,7},{5,4},{6,5},{7,6},{8,11},{9,8},{10,9... | collective-permute-start | bytes 3145736 | tf_op jit(solution)/shard_map/ppermute | solution.py:356
  102.9 1.9 fusion.31
  104.7 64.3 %collective-permute-done.18.refs_1_ = bf16[256,768]{1,0:T(8,128)(2,1)} collective-permute-done((bf16[256,768]{1,0:T(8,128)(2,1)S(1)}, bf16[256,768]{1,0:T(8,128)(2,1)}, u32[]{:S(2)}, u32[]{:S(2)}) %collective-permute-start.18) | collective-permute-done | bytes 393248 | tf_op jit(solution)/shard_map/ppermute | solution.py:356
  170.5 1.5 collective-permute-start.12
  176.4 8.3 %shard_map.160.hidden_hbm = bf16[512,1024]{1,0:T(8,128)(2,1)} custom-call(bf16[512,2048]{1,0:T(8,128)(2,1)} %bitcast.36, bf16[2048,256]{1,0:T(8,128)(2,1)} %bitcast.48, bf16[2048,256]{1,0:T(8,128)(2,1)} %bitcast.51, bf16[2048,256]{1,0:T(8,128)(2,1)} %collective-permute-done.6.refs_2_, bf16[2048,256]{1,0:T(8,128)(2,1)} %copy-done.12, ...), custom_call_target="tpu_custom_call" | custom-call | flops 4294967296 | bytes 8388608 | tf_op jit(solution)/shard_map/pallas_call | solution.py:288
  184.7 2.3 collective-permute-start.15
  187.0 9.3 %collective-permute-done.20.refs_3_ = bf16[256,768]{1,0:T(8,128)(2,1)} collective-permute-done((bf16[256,768]{1,0:T(8,128)(2,1)}, bf16[256,768]{1,0:T(8,128)(2,1)}, u32[]{:S(2)}, u32[]{:S(2)}) %collective-permute-start.20) | collective-permute-done | bytes 393248 | tf_op jit(solution)/shard_map/ppermute | solution.py:356
  196.4 3.5 %shard_map.162 = bf16[512,768]{1,0:T(8,128)(2,1)} custom-call(bf16[512,1024]{1,0:T(8,128)(2,1)} %shard_map.160.hidden_hbm, bf16[256,768]{1,0:T(8,128)(2,1)} %copy-done.2, bf16[256,768]{1,0:T(8,128)(2,1)} %collective-permute-done.18.refs_1_, bf16[256,768]{1,0:T(8,128)(2,1)} %collective-permute-done.19.refs_2_, bf16[256,768]{1,0:T(8,128)(2,1)} %collective-permute-done.20.refs_3_), custom_call_target="tpu_custom_call" | custom-call | flops 805306368 | bytes 1572864 | tf_op jit(solution)/shard_map/pallas_call | solution.py:335
  199.9 7.2 %all-to-all-start.2 = ((bf16[32,16,768]{2,1,0:T(8,128)(2,1)}), bf16[32,16,768]{2,1,0:T(8,128)(2,1)S(1)}, u32[]{:S(2)}, u32[]{:S(2)}) async-start(bf16[32,16,768]{2,1,0:T(8,128)(2,1)} %bitcast.35), calls=%async_computation.3 | async-start | bytes 1572864 | tf_op jit(solution)/shard_map/all_to_all | solution.py:454
  207.8 1.8 collective-permute-start.17
  209.7 8.0 %collective-permute-done.16.refs_6_ = bf16[128,1280]{1,0:T(8,128)(2,1)S(1)} collective-permute-done((bf16[128,1280]{1,0:T(8,128)(2,1)}, bf16[128,1280]{1,0:T(8,128)(2,1)S(1)}, u32[]{:S(2)}, u32[]{:S(2)}) %collective-permute-start.16) | collective-permute-done | bytes 327712 | tf_op jit(solution)/shard_map/ppermute | solution.py:356
  219.7 4.5 %shard_map.161 = bf16[512,1280]{1,0:T(8,128)(2,1)} custom-call(bf16[512,1024]{1,0:T(8,128)(2,1)} %shard_map.160.hidden_hbm, bf16[128,1280]{1,0:T(8,128)(2,1)} %get-tuple-element.19.refs_0_, bf16[128,1280]{1,0:T(8,128)(2,1)} %copy-done.3, bf16[128,1280]{1,0:T(8,128)(2,1)} %collective-permute-done.12.refs_2_, ...), custom_call_target="tpu_custom_call" | custom-call | flops 1342177280 | bytes 2621440 | tf_op jit(solution)/shard_map/pallas_call | solution.py:335
  224.2 7.2 %all-to-all-start.1 = ((bf16[32,16,1280]{2,1,0:T(8,128)(2,1)}), bf16[32,16,1280]{2,1,0:T(8,128)(2,1)S(1)}, u32[]{:S(2)}, u32[]{:S(2)}) async-start(bf16[32,16,1280]{2,1,0:T(8,128)(2,1)} %bitcast.34), calls=%async_computation.2 | async-start | bytes 2621440 | tf_op jit(solution)/shard_map/all_to_all | solution.py:454
  233.3 2.0 fusion.16
  235.4 16.7 %all-to-all-done.1 = bf16[32,16,1280]{2,1,0:T(8,128)(2,1)S(1)} async-done(((bf16[32,16,1280]{2,1,0:T(8,128)(2,1)}), bf16[32,16,1280]{2,1,0:T(8,128)(2,1)S(1)}, u32[]{:S(2)}, u32[]{:S(2)}) %all-to-all-start.1) | async-done | bytes 1310752 | tf_op jit(solution)/shard_map/all_to_all | solution.py:454
  (109 shorter events, 26.5 us)
Async XLA Ops:
  7.2 95.4 %copy-start = (bf16[2048,32]{0,1:T(8,128)(2,1)S(1)}, bf16[2048,32]{0,1:T(8,128)(2,1)}, u32[]{:S(2)}) copy-start(bf16[2048,32]{0,1:T(8,128)(2,1)} %param.24) | copy-start | bytes 393220
  7.2 32.8 %all-gather.2.cloned.1.call-start = ((), (), s32[]{:S(2)}) async-start(), calls=%async_computation.4 | async-start | bytes 2433024 | tf_op jit(solution)/shard_map/all_gather | solution.py:413
  11.8 220.3 %reduce-scatter.2.cloned.1.call-start = ((), (), s32[]{:S(2)}) async-start(), calls=%async_computation.5 | async-start | bytes 2621440 | tf_op jit(solution)/shard_map/reduce_scatter | solution.py:458
  11.9 11.9 %collective-permute-start = (bf16[512,256]{1,0:T(8,128)(2,1)}, bf16[512,256]{1,0:T(8,128)(2,1)S(1)}, u32[]{:S(2)}, u32[]{:S(2)}) collective-permute-start(bf16[512,256]{1,0:T(8,128)(2,1)} %q0.1), channel_id=1, source_target_pairs={{32,0},{36,4},{40,8},{44,12},{48,16},{52,20},{56,24},{60,28},{64,3... | collective-permute-start | bytes 786440 | tf_op jit(solution)/shard_map/ppermute | solution.py:419
  13.2 12.5 %collective-permute-start.1 = (bf16[512,256]{1,0:T(8,128)(2,1)}, bf16[512,256]{1,0:T(8,128)(2,1)S(1)}, u32[]{:S(2)}, u32[]{:S(2)}) collective-permute-start(bf16[512,256]{1,0:T(8,128)(2,1)} %q0.1), channel_id=1, source_target_pairs={{64,0},{68,4},{72,8},{76,12},{80,16},{84,20},{88,24},{92,28},{96,3... | collective-permute-start | bytes 786440 | tf_op jit(solution)/shard_map/ppermute | solution.py:419
  14.5 16.7 %collective-permute-start.2 = (bf16[512,256]{1,0:T(8,128)(2,1)}, bf16[512,256]{1,0:T(8,128)(2,1)S(1)}, u32[]{:S(2)}, u32[]{:S(2)}) collective-permute-start(bf16[512,256]{1,0:T(8,128)(2,1)} %q0.1), channel_id=1, source_target_pairs={{96,0},{100,4},{104,8},{108,12},{112,16},{116,20},{120,24},{124,28... | collective-permute-start | bytes 786440 | tf_op jit(solution)/shard_map/ppermute | solution.py:419
  15.8 82.4 %collective-permute-start.6 = (bf16[2048,256]{1,0:T(8,128)(2,1)}, bf16[2048,256]{1,0:T(8,128)(2,1)}, u32[]{:S(2)}, u32[]{:S(2)}) collective-permute-start(bf16[2048,256]{1,0:T(8,128)(2,1)} %bitcast.46), channel_id=1, source_target_pairs={{0,1},{1,2},{2,3},{3,0},{4,5},{5,6},{6,7},{7,4},{8,9},{9,10},{10,1... | collective-permute-start | bytes 3145736 | tf_op jit(solution)/shard_map/ppermute | solution.py:356
  17.4 81.0 %collective-permute-start.9 = (bf16[2048,256]{1,0:T(8,128)(2,1)}, bf16[2048,256]{1,0:T(8,128)(2,1)}, u32[]{:S(2)}, u32[]{:S(2)}) collective-permute-start(bf16[2048,256]{1,0:T(8,128)(2,1)} %bitcast.49), channel_id=1, source_target_pairs={{0,3},{1,0},{2,1},{3,2},{4,7},{5,4},{6,5},{7,6},{8,11},{9,8},{10,9... | collective-permute-start | bytes 3145736 | tf_op jit(solution)/shard_map/ppermute | solution.py:356
  23.8 16.2 %copy-start.16 = (bf16[512,256]{1,0:T(8,128)(2,1)}, bf16[512,256]{1,0:T(8,128)(2,1)S(1)}, u32[]{:S(2)}) copy-start(bf16[512,256]{1,0:T(8,128)(2,1)S(1)} %collective-permute-done.q1) | copy-start | bytes 786436
  25.7 14.3 %copy-start.17 = (bf16[512,256]{1,0:T(8,128)(2,1)}, bf16[512,256]{1,0:T(8,128)(2,1)S(1)}, u32[]{:S(2)}) copy-start(bf16[512,256]{1,0:T(8,128)(2,1)S(1)} %collective-permute-done.1.q2) | copy-start | bytes 786436
  63.8 8.6 %collective-permute-start.3 = (bf16[272,512]{1,0:T(8,128)(2,1)}, bf16[272,512]{1,0:T(8,128)(2,1)S(1)}, u32[]{:S(2)}, u32[]{:S(2)}) collective-permute-start(bf16[272,512]{1,0:T(8,128)(2,1)} %get-tuple-element.9), channel_id=1, source_target_pairs={{0,32},{4,36},{8,40},{12,44},{16,48},{20,52},{24,56},{28,60},{32,6... | collective-permute-start | bytes 835592 | tf_op jit(solution)/shard_map/ppermute | solution.py:424
  65.1 12.8 %collective-permute-start.4 = (bf16[272,512]{1,0:T(8,128)(2,1)}, bf16[272,512]{1,0:T(8,128)(2,1)S(1)}, u32[]{:S(2)}, u32[]{:S(2)}) collective-permute-start(bf16[272,512]{1,0:T(8,128)(2,1)} %get-tuple-element.10), channel_id=1, source_target_pairs={{0,64},{4,68},{8,72},{12,76},{16,80},{20,84},{24,88},{28,92},{32,9... | collective-permute-start | bytes 835592 | tf_op jit(solution)/shard_map/ppermute | solution.py:424
  66.4 11.5 %collective-permute-start.5 = (bf16[272,512]{1,0:T(8,128)(2,1)}, bf16[272,512]{1,0:T(8,128)(2,1)S(1)}, u32[]{:S(2)}, u32[]{:S(2)}) collective-permute-start(bf16[272,512]{1,0:T(8,128)(2,1)} %get-tuple-element.11), channel_id=1, source_target_pairs={{0,96},{4,100},{8,104},{12,108},{16,112},{20,116},{24,120},{28,124... | collective-permute-start | bytes 835592 | tf_op jit(solution)/shard_map/ppermute | solution.py:424
  84.7 90.4 %all-to-all-start = ((bf16[32,16,2048]{2,1,0:T(8,128)(2,1)}), bf16[32,16,2048]{2,1,0:T(8,128)(2,1)S(1)}, u32[]{:S(2)}, u32[]{:S(2)}) async-start(bf16[32,16,2048]{2,1,0:T(8,128)(2,1)} %bitcast.10), calls=%async_computation.1 | async-start | bytes 4194304 | tf_op jit(solution)/shard_map/all_to_all | solution.py:444
  94.9 75.0 %collective-permute-start.7 = (bf16[2048,256]{1,0:T(8,128)(2,1)}, bf16[2048,256]{1,0:T(8,128)(2,1)S(1)}, u32[]{:S(2)}, u32[]{:S(2)}) collective-permute-start(bf16[2048,256]{1,0:T(8,128)(2,1)} %bitcast.50), channel_id=1, source_target_pairs={{0,1},{1,2},{2,3},{3,0},{4,5},{5,6},{6,7},{7,4},{8,9},{9,10},{10,1... | collective-permute-start | bytes 3145736 | tf_op jit(solution)/shard_map/ppermute | solution.py:356
  96.5 74.0 %collective-permute-start.8 = (bf16[2048,256]{1,0:T(8,128)(2,1)}, bf16[2048,256]{1,0:T(8,128)(2,1)S(1)}, u32[]{:S(2)}, u32[]{:S(2)}) collective-permute-start(bf16[2048,256]{1,0:T(8,128)(2,1)} %bitcast.47), channel_id=1, source_target_pairs={{0,3},{1,0},{2,1},{3,2},{4,7},{5,4},{6,5},{7,6},{8,11},{9,8},{10,9... | collective-permute-start | bytes 3145736 | tf_op jit(solution)/shard_map/ppermute | solution.py:356
  98.2 73.7 %collective-permute-start.10 = (bf16[2048,256]{1,0:T(8,128)(2,1)}, bf16[2048,256]{1,0:T(8,128)(2,1)S(1)}, u32[]{:S(2)}, u32[]{:S(2)}) collective-permute-start(bf16[2048,256]{1,0:T(8,128)(2,1)} %collective-permute-done.6.refs_2_), channel_id=1, source_target_pairs={{0,1},{1,2},{2,3},{3,0},{4,5},{5,6},{6,7},{7,4},{8,9},{9,10},{10,1... | collective-permute-start | bytes 3145736 | tf_op jit(solution)/shard_map/ppermute | solution.py:356
  98.5 74.6 %collective-permute-start.11 = (bf16[2048,256]{1,0:T(8,128)(2,1)}, bf16[2048,256]{1,0:T(8,128)(2,1)S(1)}, u32[]{:S(2)}, u32[]{:S(2)}) collective-permute-start(bf16[2048,256]{1,0:T(8,128)(2,1)} %collective-permute-done.9.refs_5_), channel_id=1, source_target_pairs={{0,3},{1,0},{2,1},{3,2},{4,7},{5,4},{6,5},{7,6},{8,11},{9,8},{10,9... | collective-permute-start | bytes 3145736 | tf_op jit(solution)/shard_map/ppermute | solution.py:356
  102.5 82.2 %copy-start.2 = (bf16[256,768]{1,0:T(8,128)(2,1)}, bf16[256,768]{1,0:T(8,128)(2,1)S(1)}, u32[]{:S(2)}) copy-start(bf16[256,768]{1,0:T(8,128)(2,1)S(1)} %slice.41.refs_0_) | copy-start | bytes 1179652
  102.5 66.5 %collective-permute-start.18 = (bf16[256,768]{1,0:T(8,128)(2,1)S(1)}, bf16[256,768]{1,0:T(8,128)(2,1)}, u32[]{:S(2)}, u32[]{:S(2)}) collective-permute-start(bf16[256,768]{1,0:T(8,128)(2,1)S(1)} %slice.41.refs_0_), channel_id=1, source_target_pairs={{0,1},{1,2},{2,3},{3,0},{4,5},{5,6},{6,7},{7,4},{8,9},{9,10},{10,1... | collective-permute-start | bytes 1179656 | tf_op jit(solution)/shard_map/ppermute | solution.py:356
  104.7 80.0 %copy-start.3 = (bf16[128,1280]{1,0:T(8,128)(2,1)}, bf16[128,1280]{1,0:T(8,128)(2,1)S(1)}, u32[]{:S(2)}) copy-start(bf16[128,1280]{1,0:T(8,128)(2,1)S(1)} %get-tuple-element.18.refs_1_) | copy-start | bytes 983044
  169.0 15.6 %collective-permute-start.19 = (bf16[256,768]{1,0:T(8,128)(2,1)S(1)}, bf16[256,768]{1,0:T(8,128)(2,1)}, u32[]{:S(2)}, u32[]{:S(2)}) collective-permute-start(bf16[256,768]{1,0:T(8,128)(2,1)S(1)} %slice.41.refs_0_), channel_id=1, source_target_pairs={{0,3},{1,0},{2,1},{3,2},{4,7},{5,4},{6,5},{7,6},{8,11},{9,8},{10,9... | collective-permute-start | bytes 1179656 | tf_op jit(solution)/shard_map/ppermute | solution.py:356
  169.9 37.6 %collective-permute-start.14 = (bf16[128,1280]{1,0:T(8,128)(2,1)}, bf16[128,1280]{1,0:T(8,128)(2,1)}, u32[]{:S(2)}, u32[]{:S(2)}) collective-permute-start(bf16[128,1280]{1,0:T(8,128)(2,1)} %get-tuple-element.19.refs_0_), channel_id=1, source_target_pairs={{0,3},{1,0},{2,1},{3,2},{4,7},{5,4},{6,5},{7,6},{8,11},{9,8},{10,9... | collective-permute-start | bytes 983048 | tf_op jit(solution)/shard_map/ppermute | solution.py:356
  170.5 39.2 %collective-permute-start.12 = (bf16[128,1280]{1,0:T(8,128)(2,1)}, bf16[128,1280]{1,0:T(8,128)(2,1)}, u32[]{:S(2)}, u32[]{:S(2)}) collective-permute-start(bf16[128,1280]{1,0:T(8,128)(2,1)} %get-tuple-element.19.refs_0_), channel_id=1, source_target_pairs={{0,1},{1,2},{2,3},{3,0},{4,5},{5,6},{6,7},{7,4},{8,9},{9,10},{10,1... | collective-permute-start | bytes 983048 | tf_op jit(solution)/shard_map/ppermute | solution.py:356
  171.9 35.9 %collective-permute-start.13 = (bf16[128,1280]{1,0:T(8,128)(2,1)S(1)}, bf16[128,1280]{1,0:T(8,128)(2,1)}, u32[]{:S(2)}, u32[]{:S(2)}) collective-permute-start(bf16[128,1280]{1,0:T(8,128)(2,1)S(1)} %get-tuple-element.18.refs_1_), channel_id=1, source_target_pairs={{0,1},{1,2},{2,3},{3,0},{4,5},{5,6},{6,7},{7,4},{8,9},{9,10},{10,1... | collective-permute-start | bytes 983048 | tf_op jit(solution)/shard_map/ppermute | solution.py:356
  174.1 22.3 %collective-permute-start.20 = (bf16[256,768]{1,0:T(8,128)(2,1)}, bf16[256,768]{1,0:T(8,128)(2,1)}, u32[]{:S(2)}, u32[]{:S(2)}) collective-permute-start(bf16[256,768]{1,0:T(8,128)(2,1)} %collective-permute-done.18.refs_1_), channel_id=1, source_target_pairs={{0,1},{1,2},{2,3},{3,0},{4,5},{5,6},{6,7},{7,4},{8,9},{9,10},{10,1... | collective-permute-start | bytes 1179656 | tf_op jit(solution)/shard_map/ppermute | solution.py:356
  184.7 22.6 %copy-start.10 = (bf16[2048,4]{0,1:T(4,128)(2,1)S(1)}, bf16[2048,4]{0,1:T(4,128)(2,1)}, u32[]{:S(2)}) copy-start(bf16[2048,4]{0,1:T(4,128)(2,1)} %param.23) | copy-start | bytes 49156
  184.7 25.0 %collective-permute-start.15 = (bf16[128,1280]{1,0:T(8,128)(2,1)S(1)}, bf16[128,1280]{1,0:T(8,128)(2,1)S(1)}, u32[]{:S(2)}, u32[]{:S(2)}) collective-permute-start(bf16[128,1280]{1,0:T(8,128)(2,1)S(1)} %get-tuple-element.18.refs_1_), channel_id=1, source_target_pairs={{0,3},{1,0},{2,1},{3,2},{4,7},{5,4},{6,5},{7,6},{8,11},{9,8},{10,9... | collective-permute-start | bytes 983048 | tf_op jit(solution)/shard_map/ppermute | solution.py:356
  199.9 24.3 %all-to-all-start.2 = ((bf16[32,16,768]{2,1,0:T(8,128)(2,1)}), bf16[32,16,768]{2,1,0:T(8,128)(2,1)S(1)}, u32[]{:S(2)}, u32[]{:S(2)}) async-start(bf16[32,16,768]{2,1,0:T(8,128)(2,1)} %bitcast.35), calls=%async_computation.3 | async-start | bytes 1572864 | tf_op jit(solution)/shard_map/all_to_all | solution.py:454
  207.5 10.2 %collective-permute-start.16 = (bf16[128,1280]{1,0:T(8,128)(2,1)}, bf16[128,1280]{1,0:T(8,128)(2,1)S(1)}, u32[]{:S(2)}, u32[]{:S(2)}) collective-permute-start(bf16[128,1280]{1,0:T(8,128)(2,1)} %collective-permute-done.14.refs_4_), channel_id=1, source_target_pairs={{0,3},{1,0},{2,1},{3,2},{4,7},{5,4},{6,5},{7,6},{8,11},{9,8},{10,9... | collective-permute-start | bytes 983048 | tf_op jit(solution)/shard_map/ppermute | solution.py:356
  207.8 11.1 %collective-permute-start.17 = (bf16[128,1280]{1,0:T(8,128)(2,1)}, bf16[128,1280]{1,0:T(8,128)(2,1)S(1)}, u32[]{:S(2)}, u32[]{:S(2)}) collective-permute-start(bf16[128,1280]{1,0:T(8,128)(2,1)} %collective-permute-done.13.refs_3_), channel_id=1, source_target_pairs={{0,1},{1,2},{2,3},{3,0},{4,5},{5,6},{6,7},{7,4},{8,9},{9,10},{10,1... | collective-permute-start | bytes 983048 | tf_op jit(solution)/shard_map/ppermute | solution.py:356
  224.2 27.8 %all-to-all-start.1 = ((bf16[32,16,1280]{2,1,0:T(8,128)(2,1)}), bf16[32,16,1280]{2,1,0:T(8,128)(2,1)S(1)}, u32[]{:S(2)}, u32[]{:S(2)}) async-start(bf16[32,16,1280]{2,1,0:T(8,128)(2,1)} %bitcast.34), calls=%async_computation.2 | async-start | bytes 2621440 | tf_op jit(solution)/shard_map/all_to_all | solution.py:454
  (13 other events, 38.4 us)
Sparse Core Ops, SparseCore 0:
  11.9 28.0 all-gather.1
  82.8 50.4 reduce-scatter.1

commit v2 on v0

--- a/solution.py
+++ b/solution.py
@@ -303,10 +303,11 @@
     )(x, *weights)
 
 
-def down_kernel(count, hidden_hbm, *refs):
+def down_kernel(count, near_hbm, far_hbm, *refs):
     weights, (out_hbm, hidden, down, out, sems) = refs[:count], refs[count:]
     ff = down.shape[0] // count
-    pairs = [(hidden_hbm, hidden)]
+    split = near_hbm.shape[1]
+    pairs = [(near_hbm, hidden.at[:, :split]), (far_hbm, hidden.at[:, split:])]
     pairs += [(w, down.at[q * ff : (q + 1) * ff, :]) for q, w in enumerate(weights)]
     copies = [pltpu.make_async_copy(src, dst, sems.at[k]) for k, (src, dst) in enumerate(pairs)]
     for c in copies:
@@ -329,26 +330,26 @@
         c.wait()
 
 
-def down_columns(hidden, weights):
-    rows, count = hidden.shape[0], len(weights)
+def down_columns(near, far, weights):
+    rows, count = near.shape[0], len(weights)
     ff, columns = weights[0].shape
     return pl.pallas_call(
         functools.partial(down_kernel, count),
         out_shape=jax.ShapeDtypeStruct((rows, columns), jnp.bfloat16),
-        in_specs=[pl.BlockSpec(memory_space=pltpu.HBM)] * (1 + count),
+        in_specs=[pl.BlockSpec(memory_space=pltpu.HBM)] * (2 + count),
         out_specs=pl.BlockSpec(memory_space=pltpu.HBM),
         scratch_shapes=[
             pltpu.VMEM((rows, count * ff), jnp.bfloat16),
             pltpu.VMEM((count * ff, columns), jnp.bfloat16),
             pltpu.VMEM((rows, columns), jnp.bfloat16),
-            pltpu.SemaphoreType.DMA((1 + count + columns // 256,)),
+            pltpu.SemaphoreType.DMA((2 + count + columns // 256,)),
         ],
         cost_estimate=pl.CostEstimate(
             flops=2 * rows * count * ff * columns,
             bytes_accessed=2 * count * ff * columns,
             transcendentals=0,
         ),
-    )(hidden, *weights)
+    )(near, far, *weights)
 
 
 def shift(x, by):
@@ -438,14 +439,13 @@
     arrived = lax.all_to_all(outgoing, "ep", split_axis=0, concat_axis=0, tiled=True)
     arrived = arrived.reshape(slots, width_model)
 
-    hidden = hidden_units(
-        arrived, (gate, up, left_gate, left_up, right_gate, right_up, far_gate, far_up)
-    )
+    near = hidden_units(arrived, (gate, up, left_gate, left_up, right_gate, right_up))
+    far = hidden_units(arrived, (far_gate, far_up))
     mixer_term = merge(place, told, out_weight)
     mixer_term, far_low[1] = lax.optimization_barrier((mixer_term, far_low[1]))
     returned = []
     for k in range(2):
-        results = down_columns(hidden, (low[k], left_low[k], right_low[k], far_low[k]))
+        results = down_columns(near, far, (low[k], left_low[k], right_low[k], far_low[k]))
         back = lax.all_to_all(
             results.reshape(experts, capacity, -1), "ep", split_axis=0, concat_axis=0, tiled=True
         )
@@ -478,7 +478,7 @@
     return (mixer_out, moe_out.astype(jnp.bfloat16))
 
 
-SPLIT = 768
+SPLIT = 512
 
 
 def solution(mesh):

time: 255 us -> 275 us (1.078)
  waiting for transfers between devices: 125 us -> 141 us
    ppermute x12, waiting for transfers between devices: 88.5 us -> 106 us  [shift(): return lax.ppermute(x, 'tp', [(i, (i + by) % count) for i in range(count)])]
    pallas_call x1 -> x2, Pallas kernels: 8.26 us -> 11.1 us  [hidden_units(): pl.pallas_call(functools.partial(hidden_kernel, count), out_shape=jax.Sha...]
  transfers between devices with their start and end apart: 23 -> 23, of which waited for: 9 -> 8; matrix products, arithmetic and copies ran while one was open for 5% -> 4% of each run, Pallas kernels for 17% -> 17%
where the time goes in v2:
time: 275 us; the launch traced here: 274 us
  waiting for transfers between devices  141 us (51%)
  starting transfers between devices  48.9 us (18%)
  Pallas kernels  46.7 us (17%)
  between operations  14.6 us (5%)
  other arithmetic  11.4 us (4%)
  local copies, waits for them, and re-layouts  7.26 us (3%)
  matrix products  3.54 us (1%)
    ppermute x12, waiting for transfers between devices, shift(): return lax.ppermute(x, 'tp', [(i, (i + by) % count) for i in range(count)])  106 us
    all_to_all x2, waiting for transfers between devices, inner(): lax.all_to_all(results.reshape(experts, capacity, -1), 'ep', split_axis=0...  26.3 us
    pallas_call x1, Pallas kernels, attend(): pl.pallas_call(attend_kernel, out_shape=[jax.ShapeDtypeStruct((2 * DH + 1...  23.8 us
    ppermute x12, starting transfers between devices, shift(): return lax.ppermute(x, 'tp', [(i, (i + by) % count) for i in range(count)])  18.5 us
    all_to_all x1, starting transfers between devices, inner(): lax.all_to_all(outgoing, 'ep', split_axis=0, concat_axis=0, tiled=True)  11.4 us
    all_to_all x2, starting transfers between devices, inner(): lax.all_to_all(results.reshape(experts, capacity, -1), 'ep', split_axis=0...  11.2 us
    pallas_call x2, Pallas kernels, hidden_units(): pl.pallas_call(functools.partial(hidden_kernel, count), out_shape=jax.Sha...  11.1 us
    ppermute x3, waiting for transfers between devices, inner(): told.append(lax.ppermute(answers[d], 'ep', pairs))  8.79 us
  transfers between devices with their start and end apart: 23, of which 8 were waited for; matrix products, arithmetic and copies ran while one was open for 4% of the time, Pallas kernels for 17%

profile of v2, /device:TPU:0, one launch (start us, length us, event | category | flops | bytes accessed | tf_op | source)
XLA Modules:
  0.0 273.9 jit_solution(13375758194793891617)
XLA Ops:
  10.3 1.6 pad_maximum_fusion.1
  12.0 1.3 collective-permute-start
  13.3 1.3 collective-permute-start.1
  14.6 1.3 collective-permute-start.2
  17.1 2.9 %collective-permute-start.6 = (bf16[256,1536]{1,0:T(8,128)(2,1)S(1)}, bf16[256,1536]{1,0:T(8,128)(2,1)}, u32[]{:S(2)}, u32[]{:S(2)}) collective-permute-start(bf16[256,1536]{1,0:T(8,128)(2,1)S(1)} %slice.35.refs_0_), channel_id=1, source_target_pairs={{0,3},{1,0},{2,1},{3,2},{4,7},{5,4},{6,5},{7,6},{8,11},{9,8},{10,9... | collective-permute-start | bytes 2359304 | tf_op jit(solution)/shard_map/ppermute | solution.py:357
  23.2 13.7 %collective-permute-done.6.refs_2_ = bf16[256,1536]{1,0:T(8,128)(2,1)} collective-permute-done((bf16[256,1536]{1,0:T(8,128)(2,1)S(1)}, bf16[256,1536]{1,0:T(8,128)(2,1)}, u32[]{:S(2)}, u32[]{:S(2)}) %collective-permute-start.6) | collective-permute-done | bytes 786464 | tf_op jit(solution)/shard_map/ppermute | solution.py:357
  36.9 3.8 %collective-permute-start.7 = (bf16[256,1536]{1,0:T(8,128)(2,1)}, bf16[256,1536]{1,0:T(8,128)(2,1)S(1)}, u32[]{:S(2)}, u32[]{:S(2)}) collective-permute-start(bf16[256,1536]{1,0:T(8,128)(2,1)} %collective-permute-done.6.refs_2_), channel_id=1, source_target_pairs={{0,3},{1,0},{2,1},{3,2},{4,7},{5,4},{6,5},{7,6},{8,11},{9,8},{10,9... | collective-permute-start | bytes 2359304 | tf_op jit(solution)/shard_map/ppermute | solution.py:357
  40.7 23.8 %shard_map.158 = (bf16[272,512]{1,0:T(8,128)(2,1)}, bf16[272,512]{1,0:T(8,128)(2,1)}, bf16[272,512]{1,0:T(8,128)(2,1)}, bf16[272,512]{1,0:T(8,128)(2,1)}) custom-call(s32[2]{0:T(128)} %pad_add_fusion.pos_ref, bf16[512,256]{1,0:T(8,128)(2,1)} %q0.1, bf16[512,256]{1,0:T(8,128)(2,1)} %collective-permute-done.q1, bf16[512,256]{1,0:T(8,128)(2,1)} %collective-permute-done.1.q2, ...), custom_call_target="tpu_custom_call" | custom-call | flops 8999999488 | bytes 4000000 | tf_op jit(solution)/shard_map/pallas_call | solution.py:171
  64.5 1.3 collective-permute-start.3
  65.8 1.3 collective-permute-start.4
  67.1 1.3 collective-permute-start.5
  69.1 4.0 %collective-permute-done.3.p1 = bf16[272,512]{1,0:T(8,128)(2,1)S(1)} collective-permute-done((bf16[272,512]{1,0:T(8,128)(2,1)}, bf16[272,512]{1,0:T(8,128)(2,1)S(1)}, u32[]{:S(2)}, u32[]{:S(2)}) %collective-permute-start.3) | collective-permute-done | bytes 278560 | tf_op jit(solution)/shard_map/ppermute | solution.py:419
  73.1 4.8 %collective-permute-done.4.p2 = bf16[272,512]{1,0:T(8,128)(2,1)S(1)} collective-permute-done((bf16[272,512]{1,0:T(8,128)(2,1)}, bf16[272,512]{1,0:T(8,128)(2,1)S(1)}, u32[]{:S(2)}, u32[]{:S(2)}) %collective-permute-start.4) | collective-permute-done | bytes 278560 | tf_op jit(solution)/shard_map/ppermute | solution.py:419
  78.7 3.9 %shard_map.159 = bf16[512,2048]{1,0:T(8,128)(2,1)} custom-call(s32[2]{0:T(128)} %pad_add_fusion.pos_ref, bf16[272,512]{1,0:T(8,128)(2,1)} %get-tuple-element.10.p0, bf16[272,512]{1,0:T(8,128)(2,1)} %copy-done.5, bf16[272,512]{1,0:T(8,128)(2,1)} %copy-done.6, bf16[272,512]{1,0:T(8,128)(2,1)} %copy-done.7, bf16[256,2048]{1,0:T(8,128)(2,1)} %w_ref.1), custom_call_target="tpu_custom_call" | custom-call | flops 536870912 | bytes 4000000 | tf_op jit(solution)/shard_map/pallas_call | solution.py:238
  83.3 2.0 convolution_convert_fusion
  85.3 11.4 %all-to-all-start = ((bf16[32,16,2048]{2,1,0:T(8,128)(2,1)}), bf16[32,16,2048]{2,1,0:T(8,128)(2,1)S(1)}, u32[]{:S(2)}, u32[]{:S(2)}) async-start(bf16[32,16,2048]{2,1,0:T(8,128)(2,1)} %bitcast.36), calls=%async_computation.1 | async-start | bytes 4194304 | tf_op jit(solution)/shard_map/all_to_all | solution.py:439
  97.3 2.8 %collective-permute-start.11 = (bf16[2048,256]{1,0:T(8,128)(2,1)}, bf16[2048,256]{1,0:T(8,128)(2,1)}, u32[]{:S(2)}, u32[]{:S(2)}) collective-permute-start(bf16[2048,256]{1,0:T(8,128)(2,1)} %bitcast.51), channel_id=1, source_target_pairs={{0,3},{1,0},{2,1},{3,2},{4,7},{5,4},{6,5},{7,6},{8,11},{9,8},{10,9... | collective-permute-start | bytes 3145736 | tf_op jit(solution)/shard_map/ppermute | solution.py:357
  100.5 1.5 collective-permute-start.9
  102.1 36.4 %collective-permute-done.8.refs_2_ = bf16[2048,256]{1,0:T(8,128)(2,1)} collective-permute-done((bf16[2048,256]{1,0:T(8,128)(2,1)}, bf16[2048,256]{1,0:T(8,128)(2,1)}, u32[]{:S(2)}, u32[]{:S(2)}) %collective-permute-start.8) | collective-permute-done | bytes 1048608 | tf_op jit(solution)/shard_map/ppermute | solution.py:357
  138.5 3.2 %collective-permute-start.13 = (bf16[2048,256]{1,0:T(8,128)(2,1)}, bf16[2048,256]{1,0:T(8,128)(2,1)}, u32[]{:S(2)}, u32[]{:S(2)}) collective-permute-start(bf16[2048,256]{1,0:T(8,128)(2,1)} %collective-permute-done.11.refs_5_), channel_id=1, source_target_pairs={{0,3},{1,0},{2,1},{3,2},{4,7},{5,4},{6,5},{7,6},{8,11},{9,8},{10,9... | collective-permute-start | bytes 3145736 | tf_op jit(solution)/shard_map/ppermute | solution.py:357
  143.1 45.7 %collective-permute-done.15.refs_1_ = bf16[256,512]{1,0:T(8,128)(2,1)S(1)} collective-permute-done((bf16[256,512]{1,0:T(8,128)(2,1)S(1)}, bf16[256,512]{1,0:T(8,128)(2,1)S(1)}, u32[]{:S(2)}, u32[]{:S(2)}) %collective-permute-start.15) | collective-permute-done | bytes 262176 | tf_op jit(solution)/shard_map/ppermute | solution.py:357
  192.8 1.3 copy-done.1
  194.1 6.9 %shard_map.160.near_hbm = bf16[512,768]{1,0:T(8,128)(2,1)} custom-call(bf16[512,2048]{1,0:T(8,128)(2,1)} %bitcast.34, bf16[2048,256]{1,0:T(8,128)(2,1)} %bitcast.50, bf16[2048,256]{1,0:T(8,128)(2,1)} %bitcast.53, bf16[2048,256]{1,0:T(8,128)(2,1)} %collective-permute-done.8.refs_2_, bf16[2048,256]{1,0:T(8,128)(2,1)} %copy-done.21, ...), custom_call_target="tpu_custom_call" | custom-call | flops 3221225472 | bytes 6291456 | tf_op jit(solution)/shard_map/pallas_call | solution.py:288
  201.1 4.2 %shard_map.161.far_hbm = bf16[512,256]{1,0:T(8,128)(2,1)} custom-call(bf16[512,2048]{1,0:T(8,128)(2,1)} %bitcast.35, bf16[2048,256]{1,0:T(8,128)(2,1)} %collective-permute-done.12.refs_0_, bf16[2048,256]{1,0:T(8,128)(2,1)} %collective-permute-done.13.refs_1_), custom_call_target="tpu_custom_call" | custom-call | flops 1073741824 | bytes 2097152 | tf_op jit(solution)/shard_map/pallas_call | solution.py:288
  205.3 10.5 %collective-permute-done.17.refs_3_ = bf16[256,512]{1,0:T(8,128)(2,1)} collective-permute-done((bf16[256,512]{1,0:T(8,128)(2,1)S(1)}, bf16[256,512]{1,0:T(8,128)(2,1)}, u32[]{:S(2)}, u32[]{:S(2)}) %collective-permute-start.17) | collective-permute-done | bytes 262176 | tf_op jit(solution)/shard_map/ppermute | solution.py:357
  215.8 3.1 %shard_map.163 = bf16[512,512]{1,0:T(8,128)(2,1)} custom-call(bf16[512,768]{1,0:T(8,128)(2,1)} %shard_map.160.near_hbm, bf16[512,256]{1,0:T(8,128)(2,1)} %shard_map.161.far_hbm, bf16[256,512]{1,0:T(8,128)(2,1)} %copy-done.2, bf16[256,512]{1,0:T(8,128)(2,1)} %copy-done.8, bf16[256,512]{1,0:T(8,128)(2,1)} %copy-done.9, ...), custom_call_target="tpu_custom_call" | custom-call | flops 536870912 | bytes 1048576 | tf_op jit(solution)/shard_map/pallas_call | solution.py:336
  218.9 7.2 %all-to-all-start.2 = ((bf16[32,16,512]{2,1,0:T(8,128)(2,1)}), bf16[32,16,512]{2,1,0:T(8,128)(2,1)S(1)}, u32[]{:S(2)}, u32[]{:S(2)}) async-start(bf16[32,16,512]{2,1,0:T(8,128)(2,1)} %bitcast.37), calls=%async_computation.3 | async-start | bytes 1048576 | tf_op jit(solution)/shard_map/all_to_all | solution.py:449
  226.5 5.0 %shard_map.162 = bf16[512,1536]{1,0:T(8,128)(2,1)} custom-call(bf16[512,768]{1,0:T(8,128)(2,1)} %shard_map.160.near_hbm, bf16[512,256]{1,0:T(8,128)(2,1)} %shard_map.161.far_hbm, bf16[256,1536]{1,0:T(8,128)(2,1)} %copy-done.3, bf16[256,1536]{1,0:T(8,128)(2,1)} %collective-permute-done.14.refs_1_, bf16[256,1536]{1,0:T(8,128)(2,1)} %collective-permute-done.6.refs_2_, ...), custom_call_target="tpu_custom_call" | custom-call | flops 1610612736 | bytes 3145728 | tf_op jit(solution)/shard_map/pallas_call | solution.py:336
  231.5 6.2 %all-to-all-done.2 = bf16[32,16,512]{2,1,0:T(8,128)(2,1)S(1)} async-done(((bf16[32,16,512]{2,1,0:T(8,128)(2,1)}), bf16[32,16,512]{2,1,0:T(8,128)(2,1)S(1)}, u32[]{:S(2)}, u32[]{:S(2)}) %all-to-all-start.2) | async-done | bytes 524320 | tf_op jit(solution)/shard_map/all_to_all | solution.py:449
  237.7 4.0 %all-to-all-start.1 = ((bf16[32,16,1536]{2,1,0:T(8,128)(2,1)}), bf16[32,16,1536]{2,1,0:T(8,128)(2,1)S(1)}, u32[]{:S(2)}, u32[]{:S(2)}) async-start(bf16[32,16,1536]{2,1,0:T(8,128)(2,1)} %bitcast.38), calls=%async_computation.2 | async-start | bytes 3145728 | tf_op jit(solution)/shard_map/all_to_all | solution.py:449
  243.5 2.0 fusion.9
  245.5 20.1 %all-to-all-done.1 = bf16[32,16,1536]{2,1,0:T(8,128)(2,1)S(1)} async-done(((bf16[32,16,1536]{2,1,0:T(8,128)(2,1)}), bf16[32,16,1536]{2,1,0:T(8,128)(2,1)S(1)}, u32[]{:S(2)}, u32[]{:S(2)}) %all-to-all-start.1) | async-done | bytes 1572896 | tf_op jit(solution)/shard_map/all_to_all | solution.py:449
  (112 shorter events, 19.6 us)
Async XLA Ops:
  7.2 135.6 %copy-start = (bf16[2048,32]{0,1:T(8,128)(2,1)S(1)}, bf16[2048,32]{0,1:T(8,128)(2,1)}, u32[]{:S(2)}) copy-start(bf16[2048,32]{0,1:T(8,128)(2,1)} %param.24) | copy-start | bytes 393220
  7.2 15.0 %copy-start.13 = (f32[2048]{0:T(1024)S(1)}, f32[2048]{0:T(1024)}, u32[]{:S(2)}) copy-start(f32[2048]{0:T(1024)} %param.22) | copy-start | bytes 24580
  7.2 33.5 %all-gather.2.cloned.1.call-start = ((), (), s32[]{:S(2)}) async-start(), calls=%async_computation.4 | async-start | bytes 2433024 | tf_op jit(solution)/shard_map/all_gather | solution.py:408
  12.0 230.3 %reduce-scatter.2.cloned.1.call-start = ((), (), s32[]{:S(2)}) async-start(), calls=%async_computation.5 | async-start | bytes 2621440 | tf_op jit(solution)/shard_map/reduce_scatter | solution.py:453
  12.0 28.6 %collective-permute-start = (bf16[512,256]{1,0:T(8,128)(2,1)}, bf16[512,256]{1,0:T(8,128)(2,1)}, u32[]{:S(2)}, u32[]{:S(2)}) collective-permute-start(bf16[512,256]{1,0:T(8,128)(2,1)} %q0.1), channel_id=1, source_target_pairs={{32,0},{36,4},{40,8},{44,12},{48,16},{52,20},{56,24},{60,28},{64,3... | collective-permute-start | bytes 786440 | tf_op jit(solution)/shard_map/ppermute | solution.py:414
  13.3 27.3 %collective-permute-start.1 = (bf16[512,256]{1,0:T(8,128)(2,1)}, bf16[512,256]{1,0:T(8,128)(2,1)}, u32[]{:S(2)}, u32[]{:S(2)}) collective-permute-start(bf16[512,256]{1,0:T(8,128)(2,1)} %q0.1), channel_id=1, source_target_pairs={{64,0},{68,4},{72,8},{76,12},{80,16},{84,20},{88,24},{92,28},{96,3... | collective-permute-start | bytes 786440 | tf_op jit(solution)/shard_map/ppermute | solution.py:414
  14.6 26.0 %collective-permute-start.2 = (bf16[512,256]{1,0:T(8,128)(2,1)}, bf16[512,256]{1,0:T(8,128)(2,1)}, u32[]{:S(2)}, u32[]{:S(2)}) collective-permute-start(bf16[512,256]{1,0:T(8,128)(2,1)} %q0.1), channel_id=1, source_target_pairs={{96,0},{100,4},{104,8},{108,12},{112,16},{116,20},{120,24},{124,28... | collective-permute-start | bytes 786440 | tf_op jit(solution)/shard_map/ppermute | solution.py:414
  17.1 47.3 %copy-start.3 = (bf16[256,1536]{1,0:T(8,128)(2,1)}, bf16[256,1536]{1,0:T(8,128)(2,1)S(1)}, u32[]{:S(2)}) copy-start(bf16[256,1536]{1,0:T(8,128)(2,1)S(1)} %slice.35.refs_0_) | copy-start | bytes 2359300
  17.1 19.7 %collective-permute-start.6 = (bf16[256,1536]{1,0:T(8,128)(2,1)S(1)}, bf16[256,1536]{1,0:T(8,128)(2,1)}, u32[]{:S(2)}, u32[]{:S(2)}) collective-permute-start(bf16[256,1536]{1,0:T(8,128)(2,1)S(1)} %slice.35.refs_0_), channel_id=1, source_target_pairs={{0,3},{1,0},{2,1},{3,2},{4,7},{5,4},{6,5},{7,6},{8,11},{9,8},{10,9... | collective-permute-start | bytes 2359304 | tf_op jit(solution)/shard_map/ppermute | solution.py:357
  22.2 46.2 %copy-start.11 = (s32[128,2]{0,1:T(2,128)}, s32[128,2]{0,1:T(2,128)S(1)}, u32[]{:S(2)}) copy-start(s32[128,2]{0,1:T(2,128)S(1)} %dynamic-slice_add_fusion) | copy-start | bytes 3076
  36.9 45.8 %collective-permute-start.7 = (bf16[256,1536]{1,0:T(8,128)(2,1)}, bf16[256,1536]{1,0:T(8,128)(2,1)S(1)}, u32[]{:S(2)}, u32[]{:S(2)}) collective-permute-start(bf16[256,1536]{1,0:T(8,128)(2,1)} %collective-permute-done.6.refs_2_), channel_id=1, source_target_pairs={{0,3},{1,0},{2,1},{3,2},{4,7},{5,4},{6,5},{7,6},{8,11},{9,8},{10,9... | collective-permute-start | bytes 2359304 | tf_op jit(solution)/shard_map/ppermute | solution.py:357
  64.5 8.6 %collective-permute-start.3 = (bf16[272,512]{1,0:T(8,128)(2,1)}, bf16[272,512]{1,0:T(8,128)(2,1)S(1)}, u32[]{:S(2)}, u32[]{:S(2)}) collective-permute-start(bf16[272,512]{1,0:T(8,128)(2,1)} %get-tuple-element.11), channel_id=1, source_target_pairs={{0,32},{4,36},{8,40},{12,44},{16,48},{20,52},{24,56},{28,60},{32,6... | collective-permute-start | bytes 835592 | tf_op jit(solution)/shard_map/ppermute | solution.py:419
  65.8 12.1 %collective-permute-start.4 = (bf16[272,512]{1,0:T(8,128)(2,1)}, bf16[272,512]{1,0:T(8,128)(2,1)S(1)}, u32[]{:S(2)}, u32[]{:S(2)}) collective-permute-start(bf16[272,512]{1,0:T(8,128)(2,1)} %get-tuple-element.12), channel_id=1, source_target_pairs={{0,64},{4,68},{8,72},{12,76},{16,80},{20,84},{24,88},{28,92},{32,9... | collective-permute-start | bytes 835592 | tf_op jit(solution)/shard_map/ppermute | solution.py:419
  67.1 10.8 %collective-permute-start.5 = (bf16[272,512]{1,0:T(8,128)(2,1)}, bf16[272,512]{1,0:T(8,128)(2,1)S(1)}, u32[]{:S(2)}, u32[]{:S(2)}) collective-permute-start(bf16[272,512]{1,0:T(8,128)(2,1)} %get-tuple-element.13), channel_id=1, source_target_pairs={{0,96},{4,100},{8,104},{12,108},{16,112},{20,116},{24,120},{28,124... | collective-permute-start | bytes 835592 | tf_op jit(solution)/shard_map/ppermute | solution.py:419
  85.3 107.5 %all-to-all-start = ((bf16[32,16,2048]{2,1,0:T(8,128)(2,1)}), bf16[32,16,2048]{2,1,0:T(8,128)(2,1)S(1)}, u32[]{:S(2)}, u32[]{:S(2)}) async-start(bf16[32,16,2048]{2,1,0:T(8,128)(2,1)} %bitcast.36), calls=%async_computation.1 | async-start | bytes 4194304 | tf_op jit(solution)/shard_map/all_to_all | solution.py:439
  96.7 41.7 %collective-permute-start.8 = (bf16[2048,256]{1,0:T(8,128)(2,1)}, bf16[2048,256]{1,0:T(8,128)(2,1)}, u32[]{:S(2)}, u32[]{:S(2)}) collective-permute-start(bf16[2048,256]{1,0:T(8,128)(2,1)} %bitcast.48), channel_id=1, source_target_pairs={{0,1},{1,2},{2,3},{3,0},{4,5},{5,6},{6,7},{7,4},{8,9},{9,10},{10,1... | collective-permute-start | bytes 3145736 | tf_op jit(solution)/shard_map/ppermute | solution.py:357
  97.3 41.2 %collective-permute-start.11 = (bf16[2048,256]{1,0:T(8,128)(2,1)}, bf16[2048,256]{1,0:T(8,128)(2,1)}, u32[]{:S(2)}, u32[]{:S(2)}) collective-permute-start(bf16[2048,256]{1,0:T(8,128)(2,1)} %bitcast.51), channel_id=1, source_target_pairs={{0,3},{1,0},{2,1},{3,2},{4,7},{5,4},{6,5},{7,6},{8,11},{9,8},{10,9... | collective-permute-start | bytes 3145736 | tf_op jit(solution)/shard_map/ppermute | solution.py:357
  100.0 89.6 %collective-permute-start.10 = (bf16[2048,256]{1,0:T(8,128)(2,1)}, bf16[2048,256]{1,0:T(8,128)(2,1)S(1)}, u32[]{:S(2)}, u32[]{:S(2)}) collective-permute-start(bf16[2048,256]{1,0:T(8,128)(2,1)} %bitcast.49), channel_id=1, source_target_pairs={{0,3},{1,0},{2,1},{3,2},{4,7},{5,4},{6,5},{7,6},{8,11},{9,8},{10,9... | collective-permute-start | bytes 3145736 | tf_op jit(solution)/shard_map/ppermute | solution.py:357
  100.5 90.3 %collective-permute-start.9 = (bf16[2048,256]{1,0:T(8,128)(2,1)}, bf16[2048,256]{1,0:T(8,128)(2,1)S(1)}, u32[]{:S(2)}, u32[]{:S(2)}) collective-permute-start(bf16[2048,256]{1,0:T(8,128)(2,1)} %bitcast.52), channel_id=1, source_target_pairs={{0,1},{1,2},{2,3},{3,0},{4,5},{5,6},{6,7},{7,4},{8,9},{9,10},{10,1... | collective-permute-start | bytes 3145736 | tf_op jit(solution)/shard_map/ppermute | solution.py:357
  138.5 62.6 %collective-permute-start.12 = (bf16[2048,256]{1,0:T(8,128)(2,1)}, bf16[2048,256]{1,0:T(8,128)(2,1)}, u32[]{:S(2)}, u32[]{:S(2)}) collective-permute-start(bf16[2048,256]{1,0:T(8,128)(2,1)} %collective-permute-done.8.refs_2_), channel_id=1, source_target_pairs={{0,1},{1,2},{2,3},{3,0},{4,5},{5,6},{6,7},{7,4},{8,9},{9,10},{10,1... | collective-permute-start | bytes 3145736 | tf_op jit(solution)/shard_map/ppermute | solution.py:357
  138.5 62.6 %collective-permute-start.13 = (bf16[2048,256]{1,0:T(8,128)(2,1)}, bf16[2048,256]{1,0:T(8,128)(2,1)}, u32[]{:S(2)}, u32[]{:S(2)}) collective-permute-start(bf16[2048,256]{1,0:T(8,128)(2,1)} %collective-permute-done.11.refs_5_), channel_id=1, source_target_pairs={{0,3},{1,0},{2,1},{3,2},{4,7},{5,4},{6,5},{7,6},{8,11},{9,8},{10,9... | collective-permute-start | bytes 3145736 | tf_op jit(solution)/shard_map/ppermute | solution.py:357
  142.7 58.4 %copy-start.2 = (bf16[256,512]{1,0:T(8,128)(2,1)}, bf16[256,512]{1,0:T(8,128)(2,1)S(1)}, u32[]{:S(2)}) copy-start(bf16[256,512]{1,0:T(8,128)(2,1)S(1)} %slice.36.refs_0_) | copy-start | bytes 786436
  142.7 46.0 %collective-permute-start.15 = (bf16[256,512]{1,0:T(8,128)(2,1)S(1)}, bf16[256,512]{1,0:T(8,128)(2,1)S(1)}, u32[]{:S(2)}, u32[]{:S(2)}) collective-permute-start(bf16[256,512]{1,0:T(8,128)(2,1)S(1)} %slice.36.refs_0_), channel_id=1, source_target_pairs={{0,1},{1,2},{2,3},{3,0},{4,5},{5,6},{6,7},{7,4},{8,9},{9,10},{10,1... | collective-permute-start | bytes 786440 | tf_op jit(solution)/shard_map/ppermute | solution.py:357
  188.7 16.5 %copy-start.8 = (bf16[256,512]{1,0:T(8,128)(2,1)}, bf16[256,512]{1,0:T(8,128)(2,1)S(1)}, u32[]{:S(2)}) copy-start(bf16[256,512]{1,0:T(8,128)(2,1)S(1)} %collective-permute-done.15.refs_1_) | copy-start | bytes 786436
  188.7 16.5 %collective-permute-start.16 = (bf16[256,512]{1,0:T(8,128)(2,1)S(1)}, bf16[256,512]{1,0:T(8,128)(2,1)S(1)}, u32[]{:S(2)}, u32[]{:S(2)}) collective-permute-start(bf16[256,512]{1,0:T(8,128)(2,1)S(1)} %slice.36.refs_0_), channel_id=1, source_target_pairs={{0,3},{1,0},{2,1},{3,2},{4,7},{5,4},{6,5},{7,6},{8,11},{9,8},{10,9... | collective-permute-start | bytes 786440 | tf_op jit(solution)/shard_map/ppermute | solution.py:357
  189.6 36.9 %collective-permute-start.14 = (bf16[256,1536]{1,0:T(8,128)(2,1)}, bf16[256,1536]{1,0:T(8,128)(2,1)}, u32[]{:S(2)}, u32[]{:S(2)}) collective-permute-start(bf16[256,1536]{1,0:T(8,128)(2,1)} %copy-done.3), channel_id=1, source_target_pairs={{0,1},{1,2},{2,3},{3,0},{4,5},{5,6},{6,7},{7,4},{8,9},{9,10},{10,1... | collective-permute-start | bytes 2359304 | tf_op jit(solution)/shard_map/ppermute | solution.py:357
  191.8 24.1 %collective-permute-start.17 = (bf16[256,512]{1,0:T(8,128)(2,1)S(1)}, bf16[256,512]{1,0:T(8,128)(2,1)}, u32[]{:S(2)}, u32[]{:S(2)}) collective-permute-start(bf16[256,512]{1,0:T(8,128)(2,1)S(1)} %collective-permute-done.15.refs_1_), channel_id=1, source_target_pairs={{0,1},{1,2},{2,3},{3,0},{4,5},{5,6},{6,7},{7,4},{8,9},{9,10},{10,1... | collective-permute-start | bytes 786440 | tf_op jit(solution)/shard_map/ppermute | solution.py:357
  205.3 20.9 %copy-start.12 = (s32[128,2]{0,1:T(2,128)S(1)}, s32[128,2]{0,1:T(2,128)}, u32[]{:S(2)}) copy-start(s32[128,2]{0,1:T(2,128)} %copy-done.11) | copy-start | bytes 3076
  205.3 20.9 %copy-start.10 = (bf16[2048,4]{0,1:T(4,128)(2,1)S(1)}, bf16[2048,4]{0,1:T(4,128)(2,1)}, u32[]{:S(2)}) copy-start(bf16[2048,4]{0,1:T(4,128)(2,1)} %param.23) | copy-start | bytes 49156
  205.3 21.2 %copy-start.19 = (s32[128]{0:T(128)S(1)}, s32[128]{0:T(128)}, u32[]{:S(2)}) copy-start(s32[128]{0:T(128)} %get-tuple-element.21) | copy-start | bytes 1540
  218.9 18.8 %all-to-all-start.2 = ((bf16[32,16,512]{2,1,0:T(8,128)(2,1)}), bf16[32,16,512]{2,1,0:T(8,128)(2,1)S(1)}, u32[]{:S(2)}, u32[]{:S(2)}) async-start(bf16[32,16,512]{2,1,0:T(8,128)(2,1)} %bitcast.37), calls=%async_computation.3 | async-start | bytes 1048576 | tf_op jit(solution)/shard_map/all_to_all | solution.py:449
  237.7 27.9 %all-to-all-start.1 = ((bf16[32,16,1536]{2,1,0:T(8,128)(2,1)}), bf16[32,16,1536]{2,1,0:T(8,128)(2,1)S(1)}, u32[]{:S(2)}, u32[]{:S(2)}) async-start(bf16[32,16,1536]{2,1,0:T(8,128)(2,1)} %bitcast.38), calls=%async_computation.2 | async-start | bytes 3145728 | tf_op jit(solution)/shard_map/all_to_all | solution.py:449
  (14 other events, 61.6 us)
Sparse Core Ops, SparseCore 0:
  12.1 27.8 all-gather.1
  82.8 48.6 reduce-scatter.1
